TPU v7x, 256 devices: a whole 4x4x8 slice. The times are simulated.
256 devices in a mesh: dp: 4 (over y), kv: 32 (over z, x), tp: 2 (over core).
Axes of the slice: x: 4, y: 4, z: 8, core: 2. Of those that a mesh axis runs over, the one named last changes fastest.
Arguments:
- tokens: bfloat16 [1024, 4096], P('dp', ('kv', 'tp')), may hold values from -11.5 to 11.5, as said below
- gain_mix: float32 [4096], replicated, may hold values from 0.1 to 1.9
- gain_mlp: float32 [4096], replicated, may hold values from 0.1 to 1.9
- decay_rate: float32 [16], replicated, may hold values from 0.01 to 1
- w_query: bfloat16 [4096, 1024], P('kv', 'tp'), may hold values from -0.09375 to 0.09375
- w_key: bfloat16 [4096, 1024], P('kv', 'tp'), may hold values from -0.09375 to 0.09375
- w_value: bfloat16 [4096, 2048], P('kv', 'tp'), may hold values from -0.09375 to 0.09375
- w_gate: bfloat16 [4096, 2048], P('kv', 'tp'), may hold values from -0.09375 to 0.09375
- w_mix: bfloat16 [2048, 4096], P('tp', 'kv'), may hold values from -0.125 to 0.125
- w_up: bfloat16 [4096, 16384], P(None, ('kv', 'tp')), may hold values from -0.09375 to 0.09375
- w_down: bfloat16 [16384, 4096], P(('kv', 'tp')), may hold values from -0.125 to 0.125
- state: float32 [1024, 16, 64, 128], P(('dp', 'kv'), 'tp'), may hold values from -2 to 2
Outputs:
- result: bfloat16 [1024, 4096], P('dp', ('kv', 'tp'))
- new_state: float32 [1024, 16, 64, 128], P(('dp', 'kv'), 'tp')
Inputs may be any that keep to these rules, and one draw needn't show every extreme that they name: `tokens`: feature scales differ across the features.
All inputs are finite; a program needn't handle non-finite values.
Results may differ from a plain program's by a relative error of at most 0.02.
Values may be sent and summed in bfloat16 or wider, within the bound.
No kernel may reach another device: no remote copies, remote signals or barrier semaphores. Data moves between devices by JAX's collectives and lax.ppermute only.
A program may use at most 64 MiB of HBM per device.

v0:
```python
import jax
import jax.numpy as jnp
from jax import lax
from jax.sharding import Mesh
from jax.sharding import PartitionSpec as P

KV = ("kv_0", "kv_1")
KV_TP = ("kv_0", "kv_1", "tp")
DP_KV = ("dp", "kv_0", "kv_1")


EPS = 1e-06


def laid_out(parts, dim):
    shape = list(parts.shape[1:])
    shape[dim] *= parts.shape[0]
    return jnp.moveaxis(parts, 0, dim).reshape(shape)


def sent_to_all(x, axis):
    peers = lax.axis_size(axis)
    return lax.all_to_all(jnp.broadcast_to(x[None], (peers, *x.shape)), axis, 0, 0, tiled=True)


def gathered_copies(x, axis, dim):
    return laid_out(sent_to_all(x, axis), dim)


def of_everyone(x, axis):
    everything = sent_to_all(x, axis)
    return jnp.sum(everything, axis=0)


def cut_along(x, dim, peers):
    shape = x.shape
    parts = x.reshape(*shape[:dim], peers, shape[dim] // peers, *shape[dim + 1 :])
    return jnp.moveaxis(parts, dim, 0)


def sum_at_owner(x, axis, dim):
    parts = cut_along(x, dim, lax.axis_size(axis))
    arrived = lax.all_to_all(parts, axis, split_axis=0, concat_axis=0, tiled=True)
    return arrived.astype(jnp.float32).sum(axis=0)


def of_everyone_2(x, axis):
    return sent_to_all(x, axis).astype(jnp.float32).sum(axis=0)


def whole_of(x, axes, dim):
    if not axes:
        return x
    nearer = lax.all_gather(x, axes[-1], axis=dim, tiled=True)
    return whole_of(nearer, axes[:-1], dim)


def per_device(
    tokens,
    gain_mix,
    gain_mlp,
    decay_rate,
    w_query,
    w_key,
    w_value,
    w_gate,
    w_mix,
    w_up,
    w_down,
    state,
):
    seq_count, head_count, key_width, value_width = state.shape
    both_cols = gathered_copies(tokens, "tp", 1)
    col_count = both_cols.shape[1]
    col_start = lax.axis_index(KV) * col_count
    model_width = col_count * lax.axis_size(KV)
    block_f = both_cols.astype(jnp.float32)
    squares = jnp.sum(block_f * block_f, axis=1)
    row_total = of_everyone(squares, KV)
    first_scale = lax.rsqrt(row_total / model_width + EPS)
    gain_cols = lax.dynamic_slice_in_dim(gain_mix, col_start, col_count)
    normed = (block_f * first_scale[:, None] * gain_cols[None, :]).astype(jnp.bfloat16)
    own_inputs = sum_at_owner(
        jnp.concatenate(
            [
                jnp.dot(normed, weight, preferred_element_type=jnp.float32)
                for weight in (w_query, w_key, w_value, w_gate)
            ],
            axis=1,
        ).astype(jnp.bfloat16),
        KV,
        0,
    ).astype(jnp.bfloat16)
    query_end = head_count * key_width
    key_end = 2 * query_end
    value_end = key_end + head_count * value_width
    query_heads = (
        own_inputs[:, :query_end].astype(jnp.float32).reshape(seq_count, head_count, key_width)
    )
    key_heads = (
        own_inputs[:, query_end:key_end]
        .astype(jnp.float32)
        .reshape(seq_count, head_count, key_width)
    )
    key_heads = key_heads * key_width ** (-0.5)
    value_heads = (
        own_inputs[:, key_end:value_end]
        .astype(jnp.float32)
        .reshape(seq_count, head_count, value_width)
    )
    gate_heads = (
        own_inputs[:, value_end:].astype(jnp.float32).reshape(seq_count, head_count, value_width)
    )
    rates = lax.dynamic_slice_in_dim(decay_rate, lax.axis_index("tp") * head_count, head_count)
    decay = jnp.exp(-rates)[None, :, None, None]
    new_state = decay * state + key_heads[:, :, :, None] * value_heads[:, :, None, :]
    read = jnp.einsum("bhd,bhde->bhe", query_heads, new_state, precision=lax.Precision.HIGHEST)
    read = read * lax.rsqrt(jnp.mean(read * read, axis=2, keepdims=True) + EPS)
    heads_out = (
        (jax.nn.silu(gate_heads) * read)
        .reshape(seq_count, head_count * value_width)
        .astype(jnp.bfloat16)
    )
    partial_value = jnp.dot(
        gathered_copies(heads_out, KV, 0), w_mix, preferred_element_type=jnp.float32
    )
    rounded = lax.optimization_barrier(partial_value.astype(jnp.bfloat16)).astype(jnp.float32)
    mixed = of_everyone_2(rounded.astype(jnp.bfloat16), "tp").astype(jnp.float32)
    resid_block = (block_f + mixed).astype(jnp.bfloat16)
    rows_full = whole_of(resid_block, KV, 1)
    rows_f = rows_full.astype(jnp.float32)
    second_scale = lax.rsqrt(jnp.mean(rows_f * rows_f, axis=1, keepdims=True) + EPS)
    normed_mlp = (rows_f * second_scale * gain_mlp[None, :]).astype(jnp.bfloat16)
    upper = jnp.dot(normed_mlp, w_up, preferred_element_type=jnp.float32)
    hidden = jnp.square(jax.nn.relu(upper)).astype(jnp.bfloat16)
    summed = sum_at_owner(
        jnp.dot(hidden, w_down, preferred_element_type=jnp.float32).astype(jnp.bfloat16), KV_TP, 1
    )
    own_width = tokens.shape[1]
    residual_cols = lax.dynamic_slice_in_dim(
        rows_f, lax.axis_index(KV_TP) * own_width, own_width, 1
    )
    result = (residual_cols + summed).astype(jnp.bfloat16)
    return (result, new_state)


def solution(mesh):
    torus = Mesh(
        mesh.devices.reshape(mesh.shape["dp"], 8, 4, mesh.shape["tp"]), ("dp", "kv_0", "kv_1", "tp")
    )
    return jax.shard_map(
        per_device,
        mesh=torus,
        in_specs=(
            P("dp", KV_TP),
            P(),
            P(),
            P(),
            P(KV, "tp"),
            P(KV, "tp"),
            P(KV, "tp"),
            P(KV, "tp"),
            P("tp", KV),
            P(None, KV_TP),
            P(KV_TP, None),
            P(DP_KV, "tp", None, None),
        ),
        out_specs=(P("dp", KV_TP), P(DP_KV, "tp", None, None)),
        check_vma=False,
    )
```

profile of v0, /device:TPU:18, one launch (start us, length us, event | category | flops | bytes accessed | tf_op | source)
XLA Modules:
  0.0 246.2 jit_solution(14415253915606332065)
XLA Ops:
  7.2 0.9 broadcast_in_dim.8
  8.1 3.8 %all_to_all.31 = bf16[2,256,64]{1,2,0:T(8,128)(2,1)S(1)} all-to-all(bf16[2,256,64]{1,2,0:T(8,128)(2,1)S(1)} %broadcast_in_dim.8), channel_id=1, replica_groups=mesh['dp'=4,'kv_0'=8,'kv_1'=4,'tp'=2] {'tp'}, dimensions={0} | all-to-all | bytes 131072 | tf_op jit(solution)/shard_map/all_to_all | solution.py:23
  11.9 0.6 broadcast_in_dim.9
  12.6 11.6 %all-to-all-start.1 = ((f32[32,1,256]{2,1,0:T(1,128)}), f32[32,1,256]{2,1,0:T(1,128)S(1)}, u32[]{:S(2)}, u32[]{:S(2)}) async-start(f32[32,1,256]{2,1,0:T(1,128)} %broadcast_in_dim.9), calls=%async_computation.1 | async-start | bytes 65536 | tf_op jit(solution)/shard_map/all_to_all | solution.py:23
  24.6 0.8 dynamic_slice.9
  25.3 7.5 %all-to-all-done.1 = f32[32,1,256]{2,1,0:T(1,128)S(1)} async-done(((f32[32,1,256]{2,1,0:T(1,128)}), f32[32,1,256]{2,1,0:T(1,128)S(1)}, u32[]{:S(2)}, u32[]{:S(2)}) %all-to-all-start.1) | async-done | bytes 32800 | tf_op jit(solution)/shard_map/all_to_all | solution.py:23
  33.1 1.1 convolution_convert_fusion.3
  34.5 0.3 convolution_convert_fusion.1
  34.8 0.3 convolution_convert_fusion.2
  35.0 1.3 pad_maximum_fusion
  36.3 5.8 %all-to-all-start.2 = ((bf16[32,8,3072]{2,1,0:T(8,128)(2,1)}), bf16[32,8,3072]{2,1,0:T(8,128)(2,1)}, u32[]{:S(2)}, u32[]{:S(2)}) async-start(bf16[32,8,3072]{2,1,0:T(8,128)(2,1)} %pad_maximum_fusion), calls=%async_computation.2 | async-start | bytes 3145728 | tf_op jit(solution)/shard_map/all_to_all | solution.py:43
  42.3 38.6 %all-to-all-done.2 = bf16[32,8,3072]{2,1,0:T(8,128)(2,1)} async-done(((bf16[32,8,3072]{2,1,0:T(8,128)(2,1)}), bf16[32,8,3072]{2,1,0:T(8,128)(2,1)}, u32[]{:S(2)}, u32[]{:S(2)}) %all-to-all-start.2) | async-done | bytes 1572896 | tf_op jit(solution)/shard_map/all_to_all | solution.py:43
  80.8 1.6 reduce_sum.68
  82.7 2.0 multiply_add_fusion
  84.7 1.3 copy-done.1
  86.0 1.1 fusion.21
  87.2 0.9 broadcast_in_dim.10
  88.1 5.6 %all-to-all-start.3 = ((bf16[32,8,1024]{2,1,0:T(8,128)(2,1)}), bf16[32,8,1024]{2,1,0:T(8,128)(2,1)S(1)}, u32[]{:S(2)}, u32[]{:S(2)}) async-start(bf16[32,8,1024]{2,1,0:T(8,128)(2,1)} %broadcast_in_dim.10), calls=%async_computation.3 | async-start | bytes 1048576 | tf_op jit(solution)/shard_map/all_to_all | solution.py:23
  93.8 15.2 %all-to-all-done.3 = bf16[32,8,1024]{2,1,0:T(8,128)(2,1)S(1)} async-done(((bf16[32,8,1024]{2,1,0:T(8,128)(2,1)}), bf16[32,8,1024]{2,1,0:T(8,128)(2,1)S(1)}, u32[]{:S(2)}, u32[]{:S(2)}) %all-to-all-start.3) | async-done | bytes 524320 | tf_op jit(solution)/shard_map/all_to_all | solution.py:23
  109.0 0.3 convolution_convert_fusion.5
  109.3 3.8 %all_to_all.32 = bf16[2,256,128]{2,1,0:T(8,128)(2,1)S(1)} all-to-all(bf16[2,256,128]{2,1,0:T(8,128)(2,1)S(1)} %broadcast_in_dim.11), channel_id=1, replica_groups=mesh['dp'=4,'kv_0'=8,'kv_1'=4,'tp'=2] {'tp'}, dimensions={0} | all-to-all | bytes 262144 | tf_op jit(solution)/shard_map/all_to_all | solution.py:23
  113.2 12.4 %all_gather.6 = bf16[256,512]{1,0:T(8,128)(2,1)} all-gather(bf16[256,128]{1,0:T(8,128)(2,1)S(1)} %add_convert_fusion.1), channel_id=1, replica_groups=mesh['dp'=4,'kv_0'=8,'kv_1'=4,'tp'=2] {'kv_1'}, dimensions={1}, use_global_device_ids=true | all-gather | bytes 327680 | tf_op jit(solution)/shard_map/all_gather | solution.py:54
  125.6 38.7 %all-gather.2.cloned.1.call-done = bf16[256,4096]{1,0:T(8,128)(2,1)} async-done(((bf16[256,512]{1,0:T(8,128)(2,1)}), bf16[256,4096]{1,0:T(8,128)(2,1)}) %all-gather.2.cloned.1.call-update) | async-done | bytes 2097168 | tf_op jit(solution)/shard_map/all_gather | solution.py:54
  164.3 2.1 multiply_reduce_fusion
  166.4 6.0 %convolution_convert_fusion = bf16[256,4096]{1,0:T(8,128)(2,1)} fusion(bf16[256,4096]{1,0:T(8,128)(2,1)S(1)} %copy-done, bf16[4096,256]{1,0:T(8,128)(2,1)} %param.21, f32[4096]{0:T(1024)S(1)} %copy-done.6, f32[256]{0:T(256)S(1)} %add_rsqrt_fusion.1, bf16[256,4096]{1,0:T(8,128)(2,1)} %all-gather.2.cloned.1.call-done), kind=kOutput, calls=%fused_computation | convolution fusion | flops 1079181312 | bytes 8406016 | tf_op jit(solution)/shard_map/dot_general | solution.py:137
  172.4 4.1 %copy.31 = bf16[256,4096]{0,1:T(8,128)(2,1)} copy(bf16[256,4096]{1,0:T(8,128)(2,1)} %convolution_convert_fusion) | data formatting | bytes 4194304 | tf_op jit(solution)/shard_map/convert_element_type | solution.py:137
  176.5 8.0 %all-to-all-start.5 = ((bf16[64,256,64]{1,2,0:T(8,128)(2,1)}), bf16[64,256,64]{1,2,0:T(8,128)(2,1)}, u32[]{:S(2)}, u32[]{:S(2)}) async-start(bf16[64,256,64]{1,2,0:T(8,128)(2,1)} %bitcast.56), calls=%async_computation.5 | async-start | bytes 4194304 | tf_op jit(solution)/shard_map/all_to_all | solution.py:43
  184.5 4.0 %convert_element_type.92 = f32[256,4096]{1,0:T(8,128)} convert(bf16[256,4096]{1,0:T(8,128)(2,1)} %all-gather.2.cloned.1.call-done) | non-fusion elementwise | flops 1048576 | bytes 6291456 | tf_op jit(solution)/shard_map/convert_element_type | solution.py:131
  188.5 47.1 %all-to-all-done.5 = bf16[64,256,64]{1,2,0:T(8,128)(2,1)} async-done(((bf16[64,256,64]{1,2,0:T(8,128)(2,1)}), bf16[64,256,64]{1,2,0:T(8,128)(2,1)}, u32[]{:S(2)}, u32[]{:S(2)}) %all-to-all-start.5) | async-done | bytes 2097184 | tf_op jit(solution)/shard_map/all_to_all | solution.py:43
  235.6 1.9 convert_reduce_fusion
  237.6 1.0 add_convert_fusion
  238.6 0.7 copy.33
  (42 shorter events, 1.6 us)
Async XLA Ops:
  7.2 159.2 %copy-start = (bf16[256,4096]{1,0:T(8,128)(2,1)S(1)}, bf16[256,4096]{1,0:T(8,128)(2,1)}, u32[]{:S(2)}) copy-start(bf16[256,4096]{1,0:T(8,128)(2,1)} %param.22) | copy-start | bytes 6291460
  7.2 27.0 %copy-start.5 = (bf16[128,512]{1,0:T(8,128)(2,1)S(1)}, bf16[128,512]{1,0:T(8,128)(2,1)}, u32[]{:S(2)}) copy-start(bf16[128,512]{1,0:T(8,128)(2,1)} %param.16) | copy-start | bytes 393220
  7.2 27.3 %copy-start.2 = (bf16[128,1024]{1,0:T(8,128)(2,1)S(1)}, bf16[128,1024]{1,0:T(8,128)(2,1)}, u32[]{:S(2)}) copy-start(bf16[128,1024]{1,0:T(8,128)(2,1)} %param.19) | copy-start | bytes 786436
  7.2 27.5 %copy-start.3 = (bf16[128,1024]{1,0:T(8,128)(2,1)S(1)}, bf16[128,1024]{1,0:T(8,128)(2,1)}, u32[]{:S(2)}) copy-start(bf16[128,1024]{1,0:T(8,128)(2,1)} %param.18) | copy-start | bytes 786436
  12.6 20.2 %all-to-all-start.1 = ((f32[32,1,256]{2,1,0:T(1,128)}), f32[32,1,256]{2,1,0:T(1,128)S(1)}, u32[]{:S(2)}, u32[]{:S(2)}) async-start(f32[32,1,256]{2,1,0:T(1,128)} %broadcast_in_dim.9), calls=%async_computation.1 | async-start | bytes 65536 | tf_op jit(solution)/shard_map/all_to_all | solution.py:23
  36.3 5.9 %copy-start.7 = (f32[16]{0:T(128)S(1)}, f32[16]{0:T(128)}, u32[]{:S(2)}) copy-start(f32[16]{0:T(128)} %param.15) | copy-start | bytes 196
  36.3 44.5 %all-to-all-start.2 = ((bf16[32,8,3072]{2,1,0:T(8,128)(2,1)}), bf16[32,8,3072]{2,1,0:T(8,128)(2,1)}, u32[]{:S(2)}, u32[]{:S(2)}) async-start(bf16[32,8,3072]{2,1,0:T(8,128)(2,1)} %pad_maximum_fusion), calls=%async_computation.2 | async-start | bytes 3145728 | tf_op jit(solution)/shard_map/all_to_all | solution.py:43
  84.7 1.3 copy-start.1
  86.0 23.0 %copy-start.4 = (bf16[1024,128]{1,0:T(8,128)(2,1)S(1)}, bf16[1024,128]{1,0:T(8,128)(2,1)}, u32[]{:S(2)}) copy-start(bf16[1024,128]{1,0:T(8,128)(2,1)} %param.20) | copy-start | bytes 786436
  88.1 20.9 %all-to-all-start.3 = ((bf16[32,8,1024]{2,1,0:T(8,128)(2,1)}), bf16[32,8,1024]{2,1,0:T(8,128)(2,1)S(1)}, u32[]{:S(2)}, u32[]{:S(2)}) async-start(bf16[32,8,1024]{2,1,0:T(8,128)(2,1)} %broadcast_in_dim.10), calls=%async_computation.3 | async-start | bytes 1048576 | tf_op jit(solution)/shard_map/all_to_all | solution.py:23
  93.7 70.6 %all-gather.2.cloned.1.call-start = ((), (), s32[]{:S(2)}) async-start(), calls=%async_computation.6 | async-start | bytes 2359296 | tf_op jit(solution)/shard_map/all_gather | solution.py:54
  93.8 72.6 %copy-start.6 = (f32[4096]{0:T(1024)S(1)}, f32[4096]{0:T(1024)}, u32[]{:S(2)}) copy-start(f32[4096]{0:T(1024)} %param.14) | copy-start | bytes 49156
  176.5 59.2 %all-to-all-start.5 = ((bf16[64,256,64]{1,2,0:T(8,128)(2,1)}), bf16[64,256,64]{1,2,0:T(8,128)(2,1)}, u32[]{:S(2)}, u32[]{:S(2)}) async-start(bf16[64,256,64]{1,2,0:T(8,128)(2,1)} %bitcast.56), calls=%async_computation.5 | async-start | bytes 4194304 | tf_op jit(solution)/shard_map/all_to_all | solution.py:43
Sparse Core Ops, SparseCore 0:
  125.7 38.5 all-gather.1
where the time goes:
time: 247 us; the launch traced here: 246 us
  waiting for transfers between devices  147 us (60%)
  starting transfers between devices  31.1 us (13%)
  blocking collectives  20 us (8%)
  other arithmetic  14.4 us (6%)
  between operations  14.3 us (6%)
  local copies, waits for them, and re-layouts  10.1 us (4%)
  matrix products  9.24 us (4%)
    all_to_all x2, waiting for transfers between devices, sum_at_owner(): lax.all_to_all(parts, axis, split_axis=0, concat_axis=0, tiled=True)  85.7 us
    all_gather x1, waiting for transfers between devices, whole_of(): nearer = lax.all_gather(x, axes[-1], axis=dim, tiled=True)  38.7 us
    all_to_all x2, waiting for transfers between devices, sent_to_all(): lax.all_to_all(jnp.broadcast_to(x[None], (peers, *x.shape)), axis, 0, 0,...  22.6 us
    all_to_all x2, starting transfers between devices, sent_to_all(): lax.all_to_all(jnp.broadcast_to(x[None], (peers, *x.shape)), axis, 0, 0,...  17.2 us
    all_to_all x2, starting transfers between devices, sum_at_owner(): lax.all_to_all(parts, axis, split_axis=0, concat_axis=0, tiled=True)  13.8 us
    all_gather x1, blocking collectives, whole_of(): nearer = lax.all_gather(x, axes[-1], axis=dim, tiled=True)  12.4 us
    all_to_all x2, blocking collectives, sent_to_all(): lax.all_to_all(jnp.broadcast_to(x[None], (peers, *x.shape)), axis, 0, 0,...  7.62 us
    dot_general x1, matrix products, per_device(): jnp.dot(hidden, w_down, preferred_element_type=jnp.float32)  5.99 us
  transfers between devices with their start and end apart: 5, of which 5 were waited for; matrix products, arithmetic and copies ran while one was open for 2% of the time, Pallas kernels for 0%

commit v1 on v0

v1 whole, which is shorter than its diff:
```python
import jax
import jax.numpy as jnp
from jax import lax
from jax.experimental import pallas as pl
from jax.experimental.pallas import tpu as pltpu
from jax.sharding import Mesh
from jax.sharding import PartitionSpec as P

KV = ("kv_0", "kv_1")
KV_TP = ("kv_0", "kv_1", "tp")
DP_KV = ("dp", "kv_0", "kv_1")

EPS = 1e-06
F32 = jnp.float32
BF16 = jnp.bfloat16
LANES = 128


def dot(a, b):
    return jnp.dot(a, b, preferred_element_type=F32)


def kernel_call(body, outs, *args, scratch=(), smem=(), flops=0, bytes_accessed=0):
    vmem = pl.BlockSpec(memory_space=pltpu.VMEM)
    in_smem = pl.BlockSpec(memory_space=pltpu.SMEM)
    return pl.pallas_call(
        body,
        out_shape=[jax.ShapeDtypeStruct(*o) for o in outs],
        in_specs=[in_smem if i in smem else vmem for i in range(len(args))],
        out_specs=[vmem] * len(outs),
        scratch_shapes=list(scratch),
        cost_estimate=pl.CostEstimate(
            flops=flops, bytes_accessed=bytes_accessed, transcendentals=0
        ),
    )(*args)


def swap_tp(x):
    return lax.ppermute(x, "tp", [(0, 1), (1, 0)])


def inputs_kernel(place, own, other, gain, w_query, w_key, w_value, w_gate, out, both_out):
    tp = place[0]
    first, second = own[...], other[...]
    both = jnp.where(
        tp == 0,
        jnp.concatenate([first, second], axis=1).astype(F32),
        jnp.concatenate([second, first], axis=1).astype(F32),
    )
    both_out[...] = both.astype(BF16)
    squares = jnp.sum(both * both, axis=1, keepdims=True)
    scaled = (both * gain[pl.ds(place[1], 1), :]).astype(BF16)
    start = 0
    for weight in (w_query, w_key, w_value, w_gate):
        width = weight.shape[1]
        out[:, start : start + width] = dot(scaled, weight[...]).astype(BF16)
        start += width
    high = squares.astype(BF16).astype(F32)
    low = squares - high
    lane = lax.broadcasted_iota(jnp.int32, (squares.shape[0], LANES), 1)
    out[:, start : start + LANES] = jnp.where(
        lane == 0, high, jnp.where(lane == 1, low, 0.0)
    ).astype(BF16)


def retention_kernel(parts, state, decay, new_state, heads_out, read_ref, *, model_width, sizes):
    seqs, heads, key_width, value_width = sizes
    peers = parts.shape[0]
    total = parts[0].astype(F32)
    for j in range(1, peers):
        total = total + parts[j].astype(F32)
    q_end = heads * key_width
    k_end = 2 * q_end
    v_end = k_end + heads * value_width
    g_end = v_end + heads * value_width
    row_total = total[:, g_end : g_end + 1] + total[:, g_end + 1 : g_end + 2]
    scale = lax.rsqrt(row_total / model_width + EPS)

    def rounded(x):
        return (x * scale).astype(BF16).astype(F32)

    query = rounded(total[:, :q_end])
    key = rounded(total[:, q_end:k_end]) * key_width ** (-0.5)
    value = rounded(total[:, k_end:v_end])
    gate = rounded(total[:, v_end:g_end])
    query_t = query.T
    key_t = key.T
    for b in range(seqs):
        for h in range(heads):
            rows = slice(h * key_width, (h + 1) * key_width)
            cols = slice(h * value_width, (h + 1) * value_width)
            old = state[b * heads + h]
            new = decay[h : h + 1, :] * old + key_t[rows, b : b + 1] * value[b : b + 1, cols]
            new_state[b * heads + h] = new
            read_ref[b : b + 1, cols] = jnp.sum(
                query_t[rows, b : b + 1] * new, axis=0, keepdims=True
            )
    for h in range(heads):
        cols = slice(h * value_width, (h + 1) * value_width)
        read = read_ref[:, cols]
        read = read * lax.rsqrt(jnp.mean(read * read, axis=1, keepdims=True) + EPS)
        g = gate[:, cols]
        done = (g / (1.0 + jnp.exp(-g)) * read).astype(BF16)
        for j in range(peers):
            heads_out[j, :, cols] = done


def mix_kernel(place, heads, w_mix, keep, send):
    tp = place[0]
    half = keep.shape[0]
    product = dot(heads[...], w_mix[...]).astype(BF16)
    top, bottom = product[:half], product[half:]
    keep[...] = jnp.where(tp == 0, top.astype(F32), bottom.astype(F32)).astype(BF16)
    send[...] = jnp.where(tp == 0, bottom.astype(F32), top.astype(F32)).astype(BF16)


def resid_kernel(place, both, keep, received, out):
    half = keep.shape[0]
    start = pl.multiple_of(place[0] * half, half)
    mixed = keep[...].astype(F32) + received[...].astype(F32)
    resid = (both[pl.ds(start, half), :].astype(F32) + mixed).astype(BF16)
    for j in range(out.shape[0]):
        out[j] = resid


def mixer_kernel(place, mine, other, gain, w_up, w_down, keep, send, resid, *, model_width):
    tp = place[0]
    peers, half, width = mine.shape
    hidden_width = w_up.shape[1]
    squares = jnp.zeros((2 * half, width), F32)
    upper = jnp.zeros((2 * half, hidden_width), F32)
    for j in range(0, peers, 2):
        pieces = []
        for i in (j, j + 1):
            block = jnp.concatenate([mine[i], other[i]], axis=0).astype(F32)
            squares = squares + block * block
            pieces.append((block * gain[i : i + 1, :]).astype(BF16))
        upper = upper + dot(
            jnp.concatenate(pieces, axis=1), w_up[j * width : (j + 2) * width, :]
        )
    scale = lax.rsqrt(jnp.sum(squares, axis=1, keepdims=True) / model_width + EPS)
    upper = jnp.maximum(upper * scale, 0.0)
    hidden = (upper * upper).astype(BF16)
    lane = lax.broadcasted_iota(jnp.int32, (half, width), 1)
    own = jnp.where(lane < width // 2, 0, 1) == tp

    for j in range(0, peers, 2):
        pair = dot(hidden, w_down[:, j * width : (j + 2) * width])
        for i in (j, j + 1):
            cols = slice((i - j) * width, (i - j + 1) * width)
            from_mine, from_other = pair[:half, cols], pair[half:, cols]
            keep[i] = jnp.where(own, from_mine, pltpu.roll(from_other, width // 2, 1))
            send[i] = jnp.where(own, pltpu.roll(from_mine, width // 2, 1), from_other).astype(BF16)
    spot = place[1]
    resid[...] = jnp.where(
        own,
        mine[spot].astype(F32),
        pltpu.roll(other[spot].astype(F32), width // 2, 1),
    )


def result_kernel(parts, resid, out):
    half, width = resid.shape
    total = parts[0].astype(F32)
    for j in range(1, parts.shape[0]):
        total = total + parts[j].astype(F32)
    total = resid[...] + total
    out[:half, :] = total[:, : width // 2].astype(BF16)
    out[half:, :] = pltpu.roll(total, width // 2, 1)[:, : width // 2].astype(BF16)


def per_device(
    tokens,
    gain_mix,
    gain_mlp,
    decay_rate,
    w_query,
    w_key,
    w_value,
    w_gate,
    w_mix,
    w_up,
    w_down,
    state,
):
    seqs, heads, key_width, value_width = state.shape
    rows, own_cols = tokens.shape
    half = rows // 2
    cols = 2 * own_cols
    peers = lax.axis_size(KV)
    model_width = cols * peers
    tp = lax.axis_index("tp")
    kv = lax.axis_index(KV)
    place = jnp.stack([tp, kv]).astype(jnp.int32)
    qkvg = sum(w.shape[1] for w in (w_query, w_key, w_value, w_gate))
    payload, both = kernel_call(
        inputs_kernel,
        [((rows, qkvg + LANES), BF16), ((rows, cols), BF16)],
        place,
        tokens,
        swap_tp(tokens),
        gain_mix.reshape(peers, cols),
        w_query,
        w_key,
        w_value,
        w_gate,
        smem=(0,),
    )
    parts = lax.all_to_all(
        payload.reshape(peers, seqs, qkvg + LANES), KV, 0, 0, tiled=True
    )
    rates = lax.dynamic_slice_in_dim(decay_rate, tp * heads, heads)
    decay = jnp.broadcast_to(jnp.exp(-rates)[:, None], (heads, value_width))

    def retention_body(*refs):
        retention_kernel(
            *refs, model_width=model_width, sizes=(seqs, heads, key_width, value_width)
        )

    new_state, heads_out = kernel_call(
        retention_body,
        [
            ((seqs * heads, key_width, value_width), F32),
            ((peers, seqs, heads * value_width), BF16),
        ],
        parts,
        state.reshape(seqs * heads, key_width, value_width),
        decay,
        scratch=[pltpu.VMEM((seqs, heads * value_width), F32)],
    )
    all_heads = lax.all_to_all(heads_out, KV, 0, 0, tiled=True)
    keep, send = kernel_call(
        mix_kernel,
        [((half, cols), BF16)] * 2,
        place,
        all_heads.reshape(rows, heads * value_width),
        w_mix,
        smem=(0,),
    )
    (resid,) = kernel_call(
        resid_kernel,
        [((peers, half, cols), BF16)],
        place,
        both,
        keep,
        swap_tp(send),
        smem=(0,),
    )
    mine = lax.all_to_all(resid, KV, 0, 0, tiled=True)
    other = swap_tp(mine)

    def mixer_body(*refs):
        mixer_kernel(*refs, model_width=model_width)

    keep, send, own_resid = kernel_call(
        mixer_body,
        [((peers, half, cols), F32), ((peers, half, cols), BF16), ((half, cols), F32)],
        place,
        mine,
        other,
        gain_mlp.reshape(peers, cols),
        w_up,
        w_down,
        smem=(0,),
    )
    chip_sum = (keep + swap_tp(send).astype(F32)).astype(BF16)
    parts = lax.all_to_all(chip_sum, KV, 0, 0, tiled=True)
    (result,) = kernel_call(result_kernel, [((rows, own_cols), BF16)], parts, own_resid)
    return (result, new_state.reshape(state.shape))


def solution(mesh):
    torus = Mesh(
        mesh.devices.reshape(mesh.shape["dp"], 8, 4, mesh.shape["tp"]), ("dp", "kv_0", "kv_1", "tp")
    )
    return jax.shard_map(
        per_device,
        mesh=torus,
        in_specs=(
            P("dp", KV_TP),
            P(),
            P(),
            P(),
            P(KV, "tp"),
            P(KV, "tp"),
            P(KV, "tp"),
            P(KV, "tp"),
            P("tp", KV),
            P(None, KV_TP),
            P(KV_TP, None),
            P(DP_KV, "tp", None, None),
        ),
        out_specs=(P("dp", KV_TP), P(DP_KV, "tp", None, None)),
        check_vma=False,
    )
```

time: 247 us -> 180 us (0.73)
  waiting for transfers between devices: 147 us -> 47.3 us
  blocking collectives: 20 us -> 90.6 us
  Pallas kernels: 0 us -> 20.9 us
  starting transfers between devices: 31.1 us -> 11.8 us
  between operations: 14.3 us -> 0.7 us
  other arithmetic: 14.4 us -> 2.61 us
  matrix products: 9.24 us -> 0 us
  local copies, waits for them, and re-layouts: 10.1 us -> 5.84 us
    all_to_all x2 -> x3, blocking collectives: 7.62 us -> 90.6 us  [the longest x1 34 us: per_device(): mine = lax.all_to_all(resid, KV, 0, 0, tiled=True)]
    all_to_all x4 -> x1, waiting for transfers between devices: 108 us -> 39.9 us  [per_device(): lax.all_to_all(payload.reshape(peers, seqs, qkvg + LANES), KV, 0, 0, tile...]
    all_gather x1 -> x0, waiting for transfers between devices: 38.7 us -> none  [whole_of(): nearer = lax.all_gather(x, axes[-1], axis=dim, tiled=True)]
    pallas_call x0 -> x6, Pallas kernels: none -> 20.9 us  [kernel_call(): pl.pallas_call(body, out_shape=[jax.ShapeDtypeStruct(*o) for o in outs],...]
    all_to_all x4 -> x1, starting transfers between devices: 31 us -> 11.6 us  [per_device(): lax.all_to_all(payload.reshape(peers, seqs, qkvg + LANES), KV, 0, 0, tile...]
    all_gather x1 -> x0, blocking collectives: 12.4 us -> none  [whole_of(): nearer = lax.all_gather(x, axes[-1], axis=dim, tiled=True)]
    dot_general x7 -> x0, matrix products: 9.24 us -> none  [the longest x1 5.99 us: per_device(): jnp.dot(hidden, w_down, preferred_element_type=jnp.float32)]
    ppermute x0 -> x4, waiting for transfers between devices: none -> 7.45 us  [swap_tp(): return lax.ppermute(x, 'tp', [(0, 1), (1, 0)])]
  transfers between devices with their start and end apart: 5 -> 5, of which waited for: 5 -> 5; matrix products, arithmetic and copies ran while one was open for 2% -> 0% of each run, Pallas kernels for 0% -> 0%
where the time goes in v1:
time: 180 us
  blocking collectives  90.6 us (50%)
  waiting for transfers between devices  47.3 us (26%)
  Pallas kernels  20.9 us (12%)
  starting transfers between devices  11.8 us (7%)
  local copies, waits for them, and re-layouts  5.84 us (3%)
  other arithmetic  2.61 us (1%)
    all_to_all x1, waiting for transfers between devices, per_device(): lax.all_to_all(payload.reshape(peers, seqs, qkvg + LANES), KV, 0, 0, tile...  39.9 us
    all_to_all x1, blocking collectives, per_device(): mine = lax.all_to_all(resid, KV, 0, 0, tiled=True)  34 us
    all_to_all x1, blocking collectives, per_device(): parts = lax.all_to_all(chip_sum, KV, 0, 0, tiled=True)  33.8 us
    all_to_all x1, blocking collectives, per_device(): all_heads = lax.all_to_all(heads_out, KV, 0, 0, tiled=True)  22.8 us
    pallas_call x6, Pallas kernels, kernel_call(): pl.pallas_call(body, out_shape=[jax.ShapeDtypeStruct(*o) for o in outs],...  20.9 us
    all_to_all x1, starting transfers between devices, per_device(): lax.all_to_all(payload.reshape(peers, seqs, qkvg + LANES), KV, 0, 0, tile...  11.6 us
    ppermute x4, waiting for transfers between devices, swap_tp(): return lax.ppermute(x, 'tp', [(0, 1), (1, 0)])  7.45 us
    unnamed x16, local copies, waits for them, and re-layouts  5.09 us
  transfers between devices with their start and end apart: 5, of which 5 were waited for; matrix products, arithmetic and copies ran while one was open for 0% of the time, Pallas kernels for 0%

profile of v1, /device:TPU:18, one launch (start us, length us, event | category | flops | bytes accessed | tf_op | source)
XLA Modules:
  0.0 179.8 jit_solution(14033480432643917468)
XLA Ops:
  0.6 0.9 copy.15.own
  1.5 0.0 copy-start.3
  1.5 0.1 collective-permute-start
  1.6 0.6 pad_add_fusion.place.refs_0_
  2.2 0.6 collective-permute-done.other
  2.9 0.0 copy-done.3
  2.9 0.6 copy-done.4
  3.5 3.0 %shard_map.131 = (bf16[256,3200]{1,0:T(8,128)(2,1)}, bf16[256,128]{1,0:T(8,128)(2,1)}) custom-call(s32[2]{0:T(128)} %pad_add_fusion.place.refs_0_, bf16[256,64]{1,0:T(8,128)(2,1)} %copy-done.3, bf16[256,64]{1,0:T(8,128)(2,1)} %copy-done.4, f32[32,128]{1,0:T(8,128)} %bitcast.11, bf16[128,512]{1,0:T(8,128)(2,1)} %w_query.1, bf16[128,512]{1,0:T(8,128)(2,1)} %w_key.1, ...), custom_call_target="tpu_custom_call" | custom-call | tf_op jit(solution)/shard_map/pallas_call | solution.py:26
  6.5 11.6 %all-to-all-start = ((bf16[32,8,3200]{2,1,0:T(8,128)(2,1)}), bf16[32,8,3200]{2,1,0:T(8,128)(2,1)S(1)}, u32[]{:S(2)}, u32[]{:S(2)}) async-start(bf16[32,8,3200]{2,1,0:T(8,128)(2,1)} %bitcast.10), calls=%async_computation | async-start | bytes 3276800 | tf_op jit(solution)/shard_map/all_to_all | solution.py:209
  18.1 0.0 copy-done.6
  18.1 0.1 negate_exponential_fusion
  18.2 39.9 %all-to-all-done.refs_0_ = bf16[32,8,3200]{2,1,0:T(8,128)(2,1)S(1)} async-done(((bf16[32,8,3200]{2,1,0:T(8,128)(2,1)}), bf16[32,8,3200]{2,1,0:T(8,128)(2,1)S(1)}, u32[]{:S(2)}, u32[]{:S(2)}) %all-to-all-start) | async-done | bytes 1638432 | tf_op jit(solution)/shard_map/all_to_all | solution.py:209
  58.1 0.7 broadcast_in_dim.2.refs_2_
  58.8 0.4 copy-done
  59.3 4.8 %shard_map.132 = (f32[64,64,128]{2,1,0:T(8,128)}, bf16[32,8,1024]{2,1,0:T(8,128)(2,1)}) custom-call(bf16[32,8,3200]{2,1,0:T(8,128)(2,1)} %copy-done, f32[64,64,128]{2,1,0:T(8,128)} %bitcast.8, f32[8,128]{1,0:T(8,128)} %broadcast_in_dim.2.refs_2_), custom_call_target="tpu_custom_call" | custom-call | tf_op jit(solution)/shard_map/pallas_call | solution.py:26
  64.1 22.8 %all_to_all.20 = bf16[32,8,1024]{2,1,0:T(8,128)(2,1)} all-to-all(bf16[32,8,1024]{2,1,0:T(8,128)(2,1)} %get-tuple-element.13), channel_id=1, replica_groups=mesh['dp'=4,'kv_0'=8,'kv_1'=4,'tp'=2] {'kv_0','kv_1'}, dimensions={0} | all-to-all | bytes 1048576 | tf_op jit(solution)/shard_map/all_to_all | solution.py:231
  86.9 2.0 %shard_map.133 = (bf16[128,128]{1,0:T(8,128)(2,1)}, bf16[128,128]{1,0:T(8,128)(2,1)}) custom-call(s32[2]{0:T(128)} %pad_add_fusion.place.refs_0_, bf16[256,1024]{1,0:T(8,128)(2,1)} %bitcast.9, bf16[1024,128]{1,0:T(8,128)(2,1)} %w_mix.1), custom_call_target="tpu_custom_call" | custom-call | tf_op jit(solution)/shard_map/pallas_call | solution.py:26
  88.9 0.0 collective-permute-start.1
  88.9 1.4 collective-permute-done.1.received
  90.3 0.6 copy-done.5
  90.9 2.0 %shard_map.134 = bf16[32,128,128]{2,1,0:T(8,128)(2,1)} custom-call(s32[2]{0:T(128)} %pad_add_fusion.place.refs_0_, bf16[256,128]{1,0:T(8,128)(2,1)} %get-tuple-element.11.both, bf16[128,128]{1,0:T(8,128)(2,1)} %get-tuple-element.14.keep, bf16[128,128]{1,0:T(8,128)(2,1)} %copy-done.5), custom_call_target="tpu_custom_call" | custom-call | tf_op jit(solution)/shard_map/pallas_call | solution.py:26
  92.9 34.0 %all_to_all.21.refs_1_ = bf16[32,128,128]{2,1,0:T(8,128)(2,1)S(1)} all-to-all(bf16[32,128,128]{2,1,0:T(8,128)(2,1)} %shard_map.134), channel_id=1, replica_groups=mesh['dp'=4,'kv_0'=8,'kv_1'=4,'tp'=2] {'kv_0','kv_1'}, dimensions={0} | all-to-all | bytes 2097152 | tf_op jit(solution)/shard_map/all_to_all | solution.py:249
  126.9 0.0 collective-permute-start.2
  126.9 2.7 %collective-permute-done.2.refs_2_ = bf16[32,128,128]{2,1,0:T(8,128)(2,1)S(1)} collective-permute-done((bf16[32,128,128]{2,1,0:T(8,128)(2,1)S(1)}, bf16[32,128,128]{2,1,0:T(8,128)(2,1)S(1)}, u32[]{:S(2)}, u32[]{:S(2)}) %collective-permute-start.2) | collective-permute-done | bytes 1048608 | tf_op jit(solution)/shard_map/ppermute | solution.py:39
  129.5 1.0 copy-done.2
  130.5 7.0 %shard_map.135 = (f32[32,128,128]{2,1,0:T(8,128)}, bf16[32,128,128]{2,1,0:T(8,128)(2,1)}, f32[128,128]{1,0:T(8,128)}) custom-call(s32[2]{0:T(128)} %pad_add_fusion.place.refs_0_, bf16[32,128,128]{2,1,0:T(8,128)(2,1)} %copy-done.1, bf16[32,128,128]{2,1,0:T(8,128)(2,1)} %copy-done.2, f32[32,128]{1,0:T(8,128)} %bitcast.12, bf16[4096,256]{1,0:T(8,128)(2,1)} %refs_4_.1, ...), custom_call_target="tpu_custom_call" | custom-call | tf_op jit(solution)/shard_map/pallas_call | solution.py:26
  137.5 0.1 collective-permute-start.3
  137.7 2.7 %collective-permute-done.3 = bf16[32,128,128]{2,1,0:T(8,128)(2,1)S(1)} collective-permute-done((bf16[32,128,128]{2,1,0:T(8,128)(2,1)}, bf16[32,128,128]{2,1,0:T(8,128)(2,1)S(1)}, u32[]{:S(2)}, u32[]{:S(2)}) %collective-permute-start.3) | collective-permute-done | bytes 1048608 | tf_op jit(solution)/shard_map/ppermute | solution.py:39
  140.4 1.9 %add_convert_fusion = bf16[32,128,128]{2,1,0:T(8,128)(2,1)S(1)} fusion(f32[32,128,128]{2,1,0:T(8,128)} %get-tuple-element.16, bf16[32,128,128]{2,1,0:T(8,128)(2,1)S(1)} %collective-permute-done.3), kind=kLoop, calls=%fused_computation | loop fusion | flops 1572864 | bytes 4194304 | tf_op jit(solution)/shard_map/convert_element_type | solution.py:266
  142.3 33.8 %all_to_all.22.parts = bf16[32,128,128]{2,1,0:T(8,128)(2,1)} all-to-all(bf16[32,128,128]{2,1,0:T(8,128)(2,1)S(1)} %add_convert_fusion), channel_id=1, replica_groups=mesh['dp'=4,'kv_0'=8,'kv_1'=4,'tp'=2] {'kv_0','kv_1'}, dimensions={0} | all-to-all | bytes 2097152 | tf_op jit(solution)/shard_map/all_to_all | solution.py:267
  176.2 2.1 %shard_map.136 = bf16[256,64]{1,0:T(8,128)(2,1)} custom-call(bf16[32,128,128]{2,1,0:T(8,128)(2,1)} %all_to_all.22.parts, f32[128,128]{1,0:T(8,128)} %get-tuple-element.18.resid), custom_call_target="tpu_custom_call" | custom-call | tf_op jit(solution)/shard_map/pallas_call | solution.py:26
  178.2 1.5 copy.16
  (7 shorter events, 0.0 us)
Async XLA Ops:
  1.5 1.4 copy-start.3
  1.5 1.3 collective-permute-start
  2.9 0.6 copy-start.4
  3.5 14.6 %copy-start.6 = (f32[16]{0:T(128)S(1)}, f32[16]{0:T(128)}, u32[]{:S(2)}) copy-start(f32[16]{0:T(128)} %param.15) | copy-start | bytes 196
  6.5 51.6 %all-to-all-start = ((bf16[32,8,3200]{2,1,0:T(8,128)(2,1)}), bf16[32,8,3200]{2,1,0:T(8,128)(2,1)S(1)}, u32[]{:S(2)}, u32[]{:S(2)}) async-start(bf16[32,8,3200]{2,1,0:T(8,128)(2,1)} %bitcast.10), calls=%async_computation | async-start | bytes 3276800 | tf_op jit(solution)/shard_map/all_to_all | solution.py:209
  58.1 1.2 copy-start
  88.9 1.4 collective-permute-start.1
  90.3 0.6 copy-start.5
  126.9 2.7 %copy-start.1 = (bf16[32,128,128]{2,1,0:T(8,128)(2,1)}, bf16[32,128,128]{2,1,0:T(8,128)(2,1)S(1)}, u32[]{:S(2)}) copy-start(bf16[32,128,128]{2,1,0:T(8,128)(2,1)S(1)} %all_to_all.21.refs_1_) | copy-start | bytes 3145732
  126.9 2.7 %collective-permute-start.2 = (bf16[32,128,128]{2,1,0:T(8,128)(2,1)S(1)}, bf16[32,128,128]{2,1,0:T(8,128)(2,1)S(1)}, u32[]{:S(2)}, u32[]{:S(2)}) collective-permute-start(bf16[32,128,128]{2,1,0:T(8,128)(2,1)S(1)} %all_to_all.21.refs_1_), channel_id=1, source_target_pairs={{0,1},{1,0},{2,3},{3,2},{4,5},{5,4},{6,7},{7,6},{8,9},{9,8},{10,11... | collective-permute-start | bytes 3145736 | tf_op jit(solution)/shard_map/ppermute | solution.py:39
  129.5 1.0 copy-start.2
  137.5 2.9 %collective-permute-start.3 = (bf16[32,128,128]{2,1,0:T(8,128)(2,1)}, bf16[32,128,128]{2,1,0:T(8,128)(2,1)S(1)}, u32[]{:S(2)}, u32[]{:S(2)}) collective-permute-start(bf16[32,128,128]{2,1,0:T(8,128)(2,1)} %get-tuple-element.17), channel_id=1, source_target_pairs={{0,1},{1,0},{2,3},{3,2},{4,5},{5,4},{6,7},{7,6},{8,9},{9,8},{10,11... | collective-permute-start | bytes 3145736 | tf_op jit(solution)/shard_map/ppermute | solution.py:39

commit v2 on v1

--- a/solution.py
+++ b/solution.py
@@ -29,6 +29,7 @@
         in_specs=[in_smem if i in smem else vmem for i in range(len(args))],
         out_specs=[vmem] * len(outs),
         scratch_shapes=list(scratch),
+        compiler_params=pltpu.CompilerParams(vmem_limit_bytes=20 * 2**20),
         cost_estimate=pl.CostEstimate(
             flops=flops, bytes_accessed=bytes_accessed, transcendentals=0
         ),

time: 180 us -> 169 us (0.939)
  Pallas kernels: 20.9 us -> 9.62 us
  other arithmetic: 2.61 us -> 0.48 us
  local copies, waits for them, and re-layouts: 5.84 us -> 7.68 us
    pallas_call x6, Pallas kernels: 20.9 us -> 9.62 us  [kernel_call(): pl.pallas_call(body, out_shape=[jax.ShapeDtypeStruct(*o) for o in outs],...]
    unnamed x16 -> x24, local copies, waits for them, and re-layouts: 5.09 us -> 7.61 us
where the time goes in v2:
time: 169 us; the launch traced here: 168 us
  blocking collectives  90.1 us (53%)
  waiting for transfers between devices  47.4 us (28%)
  starting transfers between devices  12 us (7%)
  Pallas kernels  9.62 us (6%)
  local copies, waits for them, and re-layouts  7.68 us (5%)
    all_to_all x1, waiting for transfers between devices, per_device(): lax.all_to_all(payload.reshape(peers, seqs, qkvg + LANES), KV, 0, 0, tile...  39.9 us
    all_to_all x1, blocking collectives, per_device(): mine = lax.all_to_all(resid, KV, 0, 0, tiled=True)  33.8 us
    all_to_all x1, blocking collectives, per_device(): parts = lax.all_to_all(chip_sum, KV, 0, 0, tiled=True)  33.7 us
    all_to_all x1, blocking collectives, per_device(): all_heads = lax.all_to_all(heads_out, KV, 0, 0, tiled=True)  22.6 us
    all_to_all x1, starting transfers between devices, per_device(): lax.all_to_all(payload.reshape(peers, seqs, qkvg + LANES), KV, 0, 0, tile...  11.6 us
    pallas_call x6, Pallas kernels, kernel_call(): pl.pallas_call(body, out_shape=[jax.ShapeDtypeStruct(*o) for o in outs],...  9.62 us
    unnamed x24, local copies, waits for them, and re-layouts  7.61 us
    ppermute x4, waiting for transfers between devices, swap_tp(): return lax.ppermute(x, 'tp', [(0, 1), (1, 0)])  7.54 us
  transfers between devices with their start and end apart: 5, of which 5 were waited for; matrix products, arithmetic and copies ran while one was open for 0% of the time, Pallas kernels for 0%

profile of v2, /device:TPU:18, one launch (start us, length us, event | category | flops | bytes accessed | tf_op | source)
XLA Modules:
  0.0 168.0 jit_solution(11902070296351262040)
XLA Ops:
  0.6 0.9 copy.15.own
  1.5 0.1 collective-permute-start
  1.6 0.1 pad_add_fusion.place.refs_0_
  1.7 1.2 collective-permute-done.other
  2.8 0.9 copy-done.3
  3.8 0.9 copy-done.4
  4.7 0.9 copy-done.6
  5.7 0.9 copy-done.7
  6.6 0.7 copy-done.8
  7.3 2.3 %shard_map.131 = (bf16[256,3200]{1,0:T(8,128)(2,1)}, bf16[256,128]{1,0:T(8,128)(2,1)S(1)}) custom-call(s32[2]{0:T(128)S(1)} %pad_add_fusion.place.refs_0_, bf16[256,64]{1,0:T(8,128)(2,1)S(1)} %copy.15.own, bf16[256,64]{1,0:T(8,128)(2,1)S(1)} %collective-permute-done.other, f32[32,128]{1,0:T(8,128)S(1)} %bitcast.10, bf16[128,512]{1,0:T(8,128)(2,1)S(1)} %copy-done.6, ...), custom_call_target="tpu_custom_call" | custom-call | tf_op jit(solution)/shard_map/pallas_call | solution.py:26
  9.6 11.6 %all-to-all-start = ((bf16[32,8,3200]{2,1,0:T(8,128)(2,1)}), bf16[32,8,3200]{2,1,0:T(8,128)(2,1)S(1)}, u32[]{:S(2)}, u32[]{:S(2)}) async-start(bf16[32,8,3200]{2,1,0:T(8,128)(2,1)} %bitcast.3), calls=%async_computation | async-start | bytes 3276800 | tf_op jit(solution)/shard_map/all_to_all | solution.py:210
  21.2 0.1 negate_exponential_fusion
  21.3 39.9 %all-to-all-done.refs_0_ = bf16[32,8,3200]{2,1,0:T(8,128)(2,1)S(1)} async-done(((bf16[32,8,3200]{2,1,0:T(8,128)(2,1)}), bf16[32,8,3200]{2,1,0:T(8,128)(2,1)S(1)}, u32[]{:S(2)}, u32[]{:S(2)}) %all-to-all-start) | async-done | bytes 1638432 | tf_op jit(solution)/shard_map/all_to_all | solution.py:210
  61.2 0.1 broadcast_in_dim.2.refs_2_
  61.3 1.6 copy-done.2
  62.9 2.6 %shard_map.132 = (f32[64,64,128]{2,1,0:T(8,128)}, bf16[32,8,1024]{2,1,0:T(8,128)(2,1)S(1)}) custom-call(bf16[32,8,3200]{2,1,0:T(8,128)(2,1)S(1)} %all-to-all-done.refs_0_, f32[64,64,128]{2,1,0:T(8,128)S(1)} %bitcast.8, f32[8,128]{1,0:T(8,128)S(1)} %broadcast_in_dim.2.refs_2_), custom_call_target="tpu_custom_call" | custom-call | tf_op jit(solution)/shard_map/pallas_call | solution.py:26
  65.5 22.6 %all_to_all.20 = bf16[32,8,1024]{2,1,0:T(8,128)(2,1)S(1)} all-to-all(bf16[32,8,1024]{2,1,0:T(8,128)(2,1)S(1)} %get-tuple-element.13), channel_id=1, replica_groups=mesh['dp'=4,'kv_0'=8,'kv_1'=4,'tp'=2] {'kv_0','kv_1'}, dimensions={0} | all-to-all | bytes 1048576 | tf_op jit(solution)/shard_map/all_to_all | solution.py:232
  88.0 0.0 copy-done.5
  88.0 0.8 shard_map.133
  88.9 0.1 collective-permute-start.1
  89.0 1.2 collective-permute-done.1.received
  90.2 0.7 shard_map.134
  90.8 33.8 %all_to_all.21.refs_1_ = bf16[32,128,128]{2,1,0:T(8,128)(2,1)S(1)} all-to-all(bf16[32,128,128]{2,1,0:T(8,128)(2,1)S(1)} %shard_map.134), channel_id=1, replica_groups=mesh['dp'=4,'kv_0'=8,'kv_1'=4,'tp'=2] {'kv_0','kv_1'}, dimensions={0} | all-to-all | bytes 2097152 | tf_op jit(solution)/shard_map/all_to_all | solution.py:250
  124.6 0.0 collective-permute-start.2
  124.6 2.7 %collective-permute-done.2.refs_2_ = bf16[32,128,128]{2,1,0:T(8,128)(2,1)S(1)} collective-permute-done((bf16[32,128,128]{2,1,0:T(8,128)(2,1)S(1)}, bf16[32,128,128]{2,1,0:T(8,128)(2,1)S(1)}, u32[]{:S(2)}, u32[]{:S(2)}) %collective-permute-start.2) | collective-permute-done | bytes 1048608 | tf_op jit(solution)/shard_map/ppermute | solution.py:40
  127.3 3.0 %shard_map.135 = (f32[32,128,128]{2,1,0:T(8,128)S(1)}, bf16[32,128,128]{2,1,0:T(8,128)(2,1)S(1)}, f32[128,128]{1,0:T(8,128)S(1)}) custom-call(s32[2]{0:T(128)S(1)} %pad_add_fusion.place.refs_0_, bf16[32,128,128]{2,1,0:T(8,128)(2,1)S(1)} %all_to_all.21.refs_1_, bf16[32,128,128]{2,1,0:T(8,128)(2,1)S(1)} %collective-permute-done.2.refs_2_, ...), custom_call_target="tpu_custom_call" | custom-call | tf_op jit(solution)/shard_map/pallas_call | solution.py:26
  130.3 0.2 collective-permute-start.3
  130.5 2.5 %collective-permute-done.3 = bf16[32,128,128]{2,1,0:T(8,128)(2,1)S(1)} collective-permute-done((bf16[32,128,128]{2,1,0:T(8,128)(2,1)S(1)}, bf16[32,128,128]{2,1,0:T(8,128)(2,1)S(1)}, u32[]{:S(2)}, u32[]{:S(2)}) %collective-permute-start.3) | collective-permute-done | bytes 1048608 | tf_op jit(solution)/shard_map/ppermute | solution.py:40
  133.0 0.3 add_convert_fusion
  133.4 33.7 %all_to_all.22.parts = bf16[32,128,128]{2,1,0:T(8,128)(2,1)S(1)} all-to-all(bf16[32,128,128]{2,1,0:T(8,128)(2,1)S(1)} %add_convert_fusion), channel_id=1, replica_groups=mesh['dp'=4,'kv_0'=8,'kv_1'=4,'tp'=2] {'kv_0','kv_1'}, dimensions={0} | all-to-all | bytes 2097152 | tf_op jit(solution)/shard_map/all_to_all | solution.py:268
  167.1 0.2 shard_map.136
  167.3 0.7 copy.16
  (15 shorter events, 0.0 us)
Async XLA Ops:
  1.5 1.3 collective-permute-start
  2.8 1.0 copy-start.3
  3.8 0.9 copy-start.4
  4.7 0.9 copy-start.6
  5.7 0.9 copy-start.7
  6.6 0.7 copy-start.8
  7.3 14.0 %copy-start.10 = (f32[16]{0:T(128)S(1)}, f32[16]{0:T(128)}, u32[]{:S(2)}) copy-start(f32[16]{0:T(128)} %param.15) | copy-start | bytes 196
  9.6 51.6 %all-to-all-start = ((bf16[32,8,3200]{2,1,0:T(8,128)(2,1)}), bf16[32,8,3200]{2,1,0:T(8,128)(2,1)S(1)}, u32[]{:S(2)}, u32[]{:S(2)}) async-start(bf16[32,8,3200]{2,1,0:T(8,128)(2,1)} %bitcast.3), calls=%async_computation | async-start | bytes 3276800 | tf_op jit(solution)/shard_map/all_to_all | solution.py:210
  61.3 1.6 copy-start.2
  62.9 25.2 %copy-start.5 = (bf16[1024,128]{1,0:T(8,128)(2,1)S(1)}, bf16[1024,128]{1,0:T(8,128)(2,1)}, u32[]{:S(2)}) copy-start(bf16[1024,128]{1,0:T(8,128)(2,1)} %w_mix.1) | copy-start | bytes 786436
  65.5 61.8 %copy-start.1 = (bf16[256,4096]{1,0:T(8,128)(2,1)S(1)}, bf16[256,4096]{1,0:T(8,128)(2,1)}, u32[]{:S(2)}) copy-start(bf16[256,4096]{1,0:T(8,128)(2,1)} %refs_5_.1) | copy-start | bytes 6291460
  88.0 39.2 %copy-start = (bf16[4096,256]{1,0:T(8,128)(2,1)S(1)}, bf16[4096,256]{1,0:T(8,128)(2,1)}, u32[]{:S(2)}) copy-start(bf16[4096,256]{1,0:T(8,128)(2,1)} %refs_4_.1) | copy-start | bytes 6291460
  88.0 39.2 %copy-start.9 = (f32[4096]{0:T(1024)S(1)}, f32[4096]{0:T(1024)}, u32[]{:S(2)}) copy-start(f32[4096]{0:T(1024)} %param.14) | copy-start | bytes 49156
  88.9 1.3 collective-permute-start.1
  124.6 2.7 %collective-permute-start.2 = (bf16[32,128,128]{2,1,0:T(8,128)(2,1)S(1)}, bf16[32,128,128]{2,1,0:T(8,128)(2,1)S(1)}, u32[]{:S(2)}, u32[]{:S(2)}) collective-permute-start(bf16[32,128,128]{2,1,0:T(8,128)(2,1)S(1)} %all_to_all.21.refs_1_), channel_id=1, source_target_pairs={{0,1},{1,0},{2,3},{3,2},{4,5},{5,4},{6,7},{7,6},{8,9},{9,8},{10,11... | collective-permute-start | bytes 3145736 | tf_op jit(solution)/shard_map/ppermute | solution.py:40
  130.3 2.7 %collective-permute-start.3 = (bf16[32,128,128]{2,1,0:T(8,128)(2,1)S(1)}, bf16[32,128,128]{2,1,0:T(8,128)(2,1)S(1)}, u32[]{:S(2)}, u32[]{:S(2)}) collective-permute-start(bf16[32,128,128]{2,1,0:T(8,128)(2,1)S(1)} %get-tuple-element.17), channel_id=1, source_target_pairs={{0,1},{1,0},{2,3},{3,2},{4,5},{5,4},{6,7},{7,6},{8,9},{9,8},{10,11... | collective-permute-start | bytes 3145736 | tf_op jit(solution)/shard_map/ppermute | solution.py:40

commit v3 on v2

v3 whole, which is shorter than its diff:
```python
import jax
import jax.numpy as jnp
from jax import lax
from jax.experimental import pallas as pl
from jax.experimental.pallas import tpu as pltpu
from jax.sharding import Mesh
from jax.sharding import PartitionSpec as P

KV = ("kv_0", "kv_1")
KV_TP = ("kv_0", "kv_1", "tp")
DP_KV = ("dp", "kv_0", "kv_1")

EPS = 1e-06
F32 = jnp.float32
BF16 = jnp.bfloat16
LANES = 128


def dot(a, b):
    return jnp.dot(a, b, preferred_element_type=F32)


def kernel_call(body, outs, *args, scratch=(), hbm=(), flops=0, bytes_accessed=0):
    vmem = pl.BlockSpec(memory_space=pltpu.VMEM)
    in_hbm = pl.BlockSpec(memory_space=pltpu.HBM)
    return pl.pallas_call(
        body,
        out_shape=[jax.ShapeDtypeStruct(*o) for o in outs],
        in_specs=[in_hbm if i in hbm else vmem for i in range(len(args))],
        out_specs=[vmem] * len(outs),
        scratch_shapes=list(scratch),
        compiler_params=pltpu.CompilerParams(vmem_limit_bytes=20 * 2**20),
        cost_estimate=pl.CostEstimate(
            flops=flops, bytes_accessed=bytes_accessed, transcendentals=0
        ),
    )(*args)


def swap_tp(x):
    return lax.ppermute(x, "tp", [(0, 1), (1, 0)])


def ring_sizes():
    return lax.axis_size("kv_0"), lax.axis_size("kv_1")


def parity_order(z_size, x_size):
    return [
        (2 * zr + zb) * x_size + 2 * xr + xb
        for zb in range(2)
        for xb in range(2)
        for zr in range(z_size // 2)
        for xr in range(x_size // 2)
    ]


def square_groups(z_size, x_size):
    groups = []
    for tp in range(2):
        for zs in range(z_size // 2):
            for xs in range(x_size // 2):
                at_z = {z % 2: z for z in ((2 * zs + tp + i) % z_size for i in range(2))}
                at_x = {x % 2: x for x in ((2 * xs + tp + i) % x_size for i in range(2))}
                groups.append(
                    [
                        (at_z[zb] * x_size + at_x[xb]) * 2 + tp
                        for zb in range(2)
                        for xb in range(2)
                    ]
                )
    return groups


def parity_groups(z_size, x_size):
    order = parity_order(z_size, x_size)
    count = len(order) // 4
    return [
        [kv * 2 + tp for kv in order[c * count : (c + 1) * count]]
        for tp in range(2)
        for c in range(4)
    ]


def in_groups(x, groups):
    return lax.all_to_all(x, KV_TP, 0, 0, axis_index_groups=groups, tiled=True)


def sum_at_owner(parts):
    sizes = ring_sizes()
    peers, *rest = parts.shape
    near = in_groups(parts.reshape(4, peers // 4, *rest), square_groups(*sizes))
    total = near.reshape(4, peers // 4, *rest).astype(F32).sum(axis=0).astype(BF16)
    return in_groups(total, parity_groups(*sizes))


def gathered(copies):
    sizes = ring_sizes()
    count, *rest = copies.shape
    far = in_groups(copies, parity_groups(*sizes))
    near = in_groups(jnp.broadcast_to(far[None], (4, count, *rest)), square_groups(*sizes))
    return near.reshape(4 * count, *rest)


def inputs_kernel(
    other, own, gain, w_query, w_key, w_value, w_gate, out, both_out, *scratch, order
):
    sources = (own, gain, w_query, w_key, w_value, w_gate)
    held, sem = scratch[:-1], scratch[-1]
    copies = [
        pltpu.make_async_copy(source, dest, sem.at[i])
        for i, (source, dest) in enumerate(zip(sources, held, strict=True))
    ]
    for copy in copies:
        copy.start()
    tp = lax.axis_index("tp")
    kv = lax.axis_index(KV)
    copies[0].wait()
    first, second = held[0][...].astype(F32), other[...].astype(F32)
    both = jnp.where(
        tp == 0,
        jnp.concatenate([first, second], axis=0),
        jnp.concatenate([second, first], axis=0),
    ).T
    both_out[...] = both.astype(BF16)
    seqs = both.shape[0] // len(order)
    both = jnp.concatenate([both[i * seqs : (i + 1) * seqs] for i in order], axis=0)
    squares = jnp.sum(both * both, axis=1, keepdims=True)
    high = squares.astype(BF16).astype(F32)
    low = squares - high
    lane = lax.broadcasted_iota(jnp.int32, (squares.shape[0], LANES), 1)
    copies[1].wait()
    scaled = (both * held[1][pl.ds(kv, 1), :]).astype(BF16)
    start = 0
    for weight, copy in zip(held[2:], copies[2:], strict=True):
        copy.wait()
        width = weight.shape[1]
        out[:, start : start + width] = dot(scaled, weight[...]).astype(BF16)
        start += width
    out[:, start : start + LANES] = jnp.where(
        lane == 0, high, jnp.where(lane == 1, low, 0.0)
    ).astype(BF16)


def decay_kernel(state, rates, out):
    heads = rates.shape[0]
    decay = jnp.exp(-rates[...])
    for i in range(out.shape[0]):
        h = i % heads
        out[i] = decay[h : h + 1, :] * state[i]


def retention_kernel(parts, decayed, new_state, heads_out, read_ref, *, model_width, sizes):
    seqs, heads, key_width, value_width = sizes
    total = parts[0].astype(F32)
    for j in range(1, parts.shape[0]):
        total = total + parts[j].astype(F32)
    q_end = heads * key_width
    k_end = 2 * q_end
    v_end = k_end + heads * value_width
    g_end = v_end + heads * value_width
    row_total = total[:, g_end : g_end + 1] + total[:, g_end + 1 : g_end + 2]
    scale = lax.rsqrt(row_total / model_width + EPS)

    def rounded(x):
        return (x * scale).astype(BF16).astype(F32)

    query = rounded(total[:, :q_end])
    key = rounded(total[:, q_end:k_end]) * key_width ** (-0.5)
    value = rounded(total[:, k_end:v_end])
    gate = rounded(total[:, v_end:g_end])
    query_t = query.T
    key_t = key.T
    for b in range(seqs):
        for h in range(heads):
            rows = slice(h * key_width, (h + 1) * key_width)
            cols = slice(h * value_width, (h + 1) * value_width)
            new = decayed[b * heads + h] + key_t[rows, b : b + 1] * value[b : b + 1, cols]
            new_state[b * heads + h] = new
            read_ref[b : b + 1, cols] = jnp.sum(
                query_t[rows, b : b + 1] * new, axis=0, keepdims=True
            )
    for h in range(heads):
        cols = slice(h * value_width, (h + 1) * value_width)
        read = read_ref[:, cols]
        read = read * lax.rsqrt(jnp.mean(read * read, axis=1, keepdims=True) + EPS)
        g = gate[:, cols]
        done = (g / (1.0 + jnp.exp(-g)) * read).astype(BF16)
        for j in range(heads_out.shape[0]):
            heads_out[j, :, cols] = done


def mix_kernel(heads, w_mix, keep, send):
    tp = lax.axis_index("tp")
    half = keep.shape[0]
    product = dot(heads[...], w_mix[...]).astype(BF16)
    top, bottom = product[:half], product[half:]
    keep[...] = jnp.where(tp == 0, top.astype(F32), bottom.astype(F32)).astype(BF16)
    send[...] = jnp.where(tp == 0, bottom.astype(F32), top.astype(F32)).astype(BF16)


def resid_kernel(both, keep, received, out):
    half = keep.shape[0]
    start = pl.multiple_of(lax.axis_index("tp") * half, half)
    mixed = keep[...].astype(F32) + received[...].astype(F32)
    resid = (both[pl.ds(start, half), :].astype(F32) + mixed).astype(BF16)
    for j in range(out.shape[0]):
        out[j] = resid


def mixer_kernel(mine, other, gain, w_up, w_down, keep, send, resid, *, model_width, order):
    tp = lax.axis_index("tp")
    kv = lax.axis_index(KV)
    peers, half, width = mine.shape
    hidden_width = w_up.shape[1]
    lane = lax.broadcasted_iota(jnp.int32, (half, width), 1)
    own = jnp.where(lane < width // 2, 0, 1) == tp
    squares = jnp.zeros((2 * half, width), F32)
    upper = jnp.zeros((2 * half, hidden_width), F32)
    own_resid = jnp.zeros((half, width), F32)
    for j in range(0, peers, 2):
        pieces = []
        for i in (j, j + 1):
            block = jnp.concatenate([mine[i], other[i]], axis=0).astype(F32)
            squares = squares + block * block
            pieces.append((block * gain[order[i] : order[i] + 1, :]).astype(BF16))
            place = jnp.where(kv == order[i], 1, 0)
            resid_here = jnp.where(
                own, block[:half], pltpu.roll(block[half:], width // 2, 1)
            )
            own_resid = jnp.where(place == 1, resid_here, own_resid)
        weights = [w_up[order[i] * width : (order[i] + 1) * width, :] for i in (j, j + 1)]
        upper = upper + dot(
            jnp.concatenate(pieces, axis=1), jnp.concatenate(weights, axis=0)
        )
    resid[...] = own_resid
    scale = lax.rsqrt(jnp.sum(squares, axis=1, keepdims=True) / model_width + EPS)
    upper = jnp.maximum(upper * scale, 0.0)
    hidden = (upper * upper).astype(BF16)
    for j in range(0, peers, 2):
        weights = [w_down[:, order[i] * width : (order[i] + 1) * width] for i in (j, j + 1)]
        pair = dot(hidden, jnp.concatenate(weights, axis=1))
        for i in (j, j + 1):
            cols = slice((i - j) * width, (i - j + 1) * width)
            from_mine, from_other = pair[:half, cols], pair[half:, cols]
            keep[i] = jnp.where(own, from_mine, pltpu.roll(from_other, width // 2, 1))
            send[i] = jnp.where(own, pltpu.roll(from_mine, width // 2, 1), from_other).astype(BF16)


def result_kernel(parts, resid, out):
    half, width = resid.shape
    total = parts[0].astype(F32)
    for j in range(1, parts.shape[0]):
        total = total + parts[j].astype(F32)
    total = (resid[...] + total).T
    out[:, :half] = total[: width // 2].astype(BF16)
    out[:, half:] = total[width // 2 :].astype(BF16)


def per_device(
    tokens,
    gain_mix,
    gain_mlp,
    decay_rate,
    w_query,
    w_key,
    w_value,
    w_gate,
    w_mix,
    w_up,
    w_down,
    state,
):
    seqs, heads, key_width, value_width = state.shape
    rows, own_cols = tokens.shape
    half = rows // 2
    cols = 2 * own_cols
    peers = lax.axis_size(KV)
    model_width = cols * peers
    order = parity_order(*ring_sizes())
    qkvg = sum(w.shape[1] for w in (w_query, w_key, w_value, w_gate))
    tokens_t = tokens.T

    def inputs_body(*refs):
        inputs_kernel(*refs, order=order)

    sources = [
        pltpu.with_memory_space_constraint(x, pltpu.HBM)
        for x in (tokens_t, gain_mix.reshape(peers, cols), w_query, w_key, w_value, w_gate)
    ]
    payload, both = kernel_call(
        inputs_body,
        [((rows, qkvg + LANES), BF16), ((rows, cols), BF16)],
        swap_tp(tokens_t),
        *sources,
        hbm=range(1, 7),
        scratch=[
            *(pltpu.VMEM(s.shape, s.dtype) for s in sources),
            pltpu.SemaphoreType.DMA((len(sources),)),
        ],
    )
    parts = sum_at_owner(payload.reshape(peers, seqs, qkvg + LANES))
    rates = lax.dynamic_slice_in_dim(decay_rate, lax.axis_index("tp") * heads, heads)
    (decayed,) = kernel_call(
        decay_kernel,
        [((seqs * heads, key_width, value_width), F32)],
        state.reshape(seqs * heads, key_width, value_width),
        jnp.broadcast_to(rates[:, None], (heads, value_width)),
        flops=10**7,
        bytes_accessed=2**23,
    )

    def retention_body(*refs):
        retention_kernel(
            *refs, model_width=model_width, sizes=(seqs, heads, key_width, value_width)
        )

    new_state, heads_out = kernel_call(
        retention_body,
        [
            ((seqs * heads, key_width, value_width), F32),
            ((peers, seqs, heads * value_width), BF16),
        ],
        parts,
        decayed,
        scratch=[pltpu.VMEM((seqs, heads * value_width), F32)],
    )
    all_heads = lax.all_to_all(heads_out, KV, 0, 0, tiled=True)
    keep, send = kernel_call(
        mix_kernel,
        [((half, cols), BF16)] * 2,
        all_heads.reshape(rows, heads * value_width),
        w_mix,
    )
    (resid,) = kernel_call(
        resid_kernel, [((peers // 4, half, cols), BF16)], both, keep, swap_tp(send)
    )
    mine = gathered(resid)
    other = swap_tp(mine)

    def mixer_body(*refs):
        mixer_kernel(*refs, model_width=model_width, order=order)

    keep, send, own_resid = kernel_call(
        mixer_body,
        [((peers, half, cols), F32), ((peers, half, cols), BF16), ((half, cols), F32)],
        mine,
        other,
        gain_mlp.reshape(peers, cols),
        w_up,
        w_down,
    )
    chip_sum = (keep + swap_tp(send).astype(F32)).astype(BF16)
    parts = sum_at_owner(chip_sum)
    (result_t,) = kernel_call(result_kernel, [((own_cols, rows), BF16)], parts, own_resid)
    return (result_t.T, new_state.reshape(state.shape))


def solution(mesh):
    torus = Mesh(
        mesh.devices.reshape(mesh.shape["dp"], 8, 4, mesh.shape["tp"]), ("dp", "kv_0", "kv_1", "tp")
    )
    return jax.shard_map(
        per_device,
        mesh=torus,
        in_specs=(
            P("dp", KV_TP),
            P(),
            P(),
            P(),
            P(KV, "tp"),
            P(KV, "tp"),
            P(KV, "tp"),
            P(KV, "tp"),
            P("tp", KV),
            P(None, KV_TP),
            P(KV_TP, None),
            P(DP_KV, "tp", None, None),
        ),
        out_specs=(P("dp", KV_TP), P(DP_KV, "tp", None, None)),
        check_vma=False,
    )
```

time: 169 us -> 144 us (0.85); the launches traced: 168 us -> 141 us
  waiting for transfers between devices: 47.4 us -> 20.4 us
  blocking collectives: 90.1 us -> 97.2 us
  local copies, waits for them, and re-layouts: 7.68 us -> 1.99 us
    all_to_all x1, waiting for transfers between devices: 39.9 us -> 13.2 us  [in_groups(): return lax.all_to_all(x, KV_TP, 0, 0, axis_index_groups=groups, tiled=True)]
    all_to_all x2 -> x5, blocking collectives: 67.5 us -> 74.1 us  [in_groups(): return lax.all_to_all(x, KV_TP, 0, 0, axis_index_groups=groups, tiled=True)]
    unnamed x24 -> x12, local copies, waits for them, and re-layouts: 7.61 us -> 1.61 us
    all_to_all x1, starting transfers between devices: 11.6 us -> 9.13 us  [in_groups(): return lax.all_to_all(x, KV_TP, 0, 0, axis_index_groups=groups, tiled=True)]
    pallas_call x6 -> x7, Pallas kernels: 9.62 us -> 8.36 us  [kernel_call(): pl.pallas_call(body, out_shape=[jax.ShapeDtypeStruct(*o) for o in outs],...]
where the time goes in v3:
time: 144 us; the launch traced here: 141 us
  blocking collectives  97.2 us (68%)
  waiting for transfers between devices  20.4 us (14%)
  starting transfers between devices  10.6 us (7%)
  Pallas kernels  8.36 us (6%)
  local copies, waits for them, and re-layouts  1.99 us (1%)
  other arithmetic  1.65 us (1%)
    all_to_all x5, blocking collectives, in_groups(): return lax.all_to_all(x, KV_TP, 0, 0, axis_index_groups=groups, tiled=True)  74.1 us
    all_to_all x1, blocking collectives, per_device(): all_heads = lax.all_to_all(heads_out, KV, 0, 0, tiled=True)  23.1 us
    all_to_all x1, waiting for transfers between devices, in_groups(): return lax.all_to_all(x, KV_TP, 0, 0, axis_index_groups=groups, tiled=True)  13.2 us
    all_to_all x1, starting transfers between devices, in_groups(): return lax.all_to_all(x, KV_TP, 0, 0, axis_index_groups=groups, tiled=True)  9.13 us
    pallas_call x7, Pallas kernels, kernel_call(): pl.pallas_call(body, out_shape=[jax.ShapeDtypeStruct(*o) for o in outs],...  8.36 us
    ppermute x4, waiting for transfers between devices, swap_tp(): return lax.ppermute(x, 'tp', [(0, 1), (1, 0)])  7.17 us
  transfers between devices with their start and end apart: 5, of which 5 were waited for; matrix products, arithmetic and copies ran while one was open for 0% of the time, Pallas kernels for 0%

profile of v3, /device:TPU:18, one launch (start us, length us, event | category | flops | bytes accessed | tf_op | source)
XLA Modules:
  0.0 140.8 jit_solution(2311247949229110292)
XLA Ops:
  0.6 0.1 collective-permute-start
  0.7 1.4 collective-permute-done.refs_0_
  2.1 2.0 %shard_map.131 = (bf16[256,3200]{1,0:T(8,128)(2,1)S(1)}, bf16[256,128]{1,0:T(8,128)(2,1)S(1)}) custom-call(bf16[64,256]{1,0:T(8,128)(2,1)S(1)} %collective-permute-done.refs_0_, bf16[64,256]{1,0:T(8,128)(2,1)} %bitcast.19, f32[32,128]{1,0:T(8,128)} %bitcast.20, bf16[128,512]{1,0:T(8,128)(2,1)} %refs_3_.2, bf16[128,512]{1,0:T(8,128)(2,1)} %refs_4_.2, ...), custom_call_target="tpu_custom_call" | custom-call | tf_op jit(solution)/shard_map/pallas_call | solution.py:26
  4.2 16.4 %all_to_all.35 = bf16[4,8,8,3200]{3,2,1,0:T(8,128)(2,1)S(1)} all-to-all(bf16[4,8,8,3200]{3,2,1,0:T(8,128)(2,1)S(1)} %bitcast.14), channel_id=1, replica_groups={{0,2,8,10},{4,6,12,14},{16,18,24,26},{20,22,28,30},{32,34,40,42},{36,38..., dimensions={0} | all-to-all | bytes 3276800 | tf_op jit(solution)/shard_map/all_to_all | solution.py:85
  20.6 1.1 reduce_sum.24
  21.7 9.1 %all-to-all-start.1 = ((bf16[8,8,3200]{2,1,0:T(8,128)(2,1)}), bf16[8,8,3200]{2,1,0:T(8,128)(2,1)S(1)}, u32[]{:S(2)}, u32[]{:S(2)}) async-start(bf16[8,8,3200]{2,1,0:T(8,128)(2,1)} %reduce_sum.24), calls=%async_computation.1 | async-start | bytes 819200 | tf_op jit(solution)/shard_map/all_to_all | solution.py:85
  30.9 0.0 copy-done.5
  30.9 0.1 dynamic_slice.3
  30.9 0.1 broadcast_in_dim.4.rates
  31.0 1.6 %copy-done.2 = f32[8,8,64,128]{3,2,1,0:T(8,128)S(1)} copy-done((f32[8,8,64,128]{3,2,1,0:T(8,128)S(1)}, f32[8,8,64,128]{3,2,1,0:T(8,128)}, u32[]{:S(2)}) %copy-start.2) | copy-done | bytes 2097176
  32.6 0.1 shard_map.132.refs_1_
  32.8 0.0 copy-start.3
  32.8 13.2 %all-to-all-done.1.refs_0_ = bf16[8,8,3200]{2,1,0:T(8,128)(2,1)S(1)} async-done(((bf16[8,8,3200]{2,1,0:T(8,128)(2,1)}), bf16[8,8,3200]{2,1,0:T(8,128)(2,1)S(1)}, u32[]{:S(2)}, u32[]{:S(2)}) %all-to-all-start.1) | async-done | bytes 409632 | tf_op jit(solution)/shard_map/all_to_all | solution.py:85
  46.0 2.5 %shard_map.133 = (f32[64,64,128]{2,1,0:T(8,128)}, bf16[32,8,1024]{2,1,0:T(8,128)(2,1)S(1)}) custom-call(bf16[8,8,3200]{2,1,0:T(8,128)(2,1)S(1)} %all-to-all-done.1.refs_0_, f32[64,64,128]{2,1,0:T(8,128)S(1)} %shard_map.132.refs_1_), custom_call_target="tpu_custom_call" | custom-call | tf_op jit(solution)/shard_map/pallas_call | solution.py:26
  48.5 23.1 %all_to_all.36 = bf16[32,8,1024]{2,1,0:T(8,128)(2,1)S(1)} all-to-all(bf16[32,8,1024]{2,1,0:T(8,128)(2,1)S(1)} %get-tuple-element.13), channel_id=1, replica_groups=mesh['dp'=4,'kv_0'=8,'kv_1'=4,'tp'=2] {'kv_0','kv_1'}, dimensions={0} | all-to-all | bytes 1048576 | tf_op jit(solution)/shard_map/all_to_all | solution.py:327
  71.6 0.3 shard_map.134
  71.9 0.1 collective-permute-start.1
  72.0 1.2 collective-permute-done.1.received
  73.2 14.9 %all_to_all.37 = bf16[8,128,128]{2,1,0:T(8,128)(2,1)S(1)} all-to-all(bf16[8,128,128]{2,1,0:T(8,128)(2,1)S(1)} %shard_map.135), channel_id=1, replica_groups={{0,4,16,20,32,36,48,52},{2,6,18,22,34,38,50,54},{8,12,24,28,40,44,56,60..., dimensions={0} | all-to-all | bytes 524288 | tf_op jit(solution)/shard_map/all_to_all | solution.py:85
  88.1 0.2 broadcast_in_dim.5
  88.3 13.8 %all_to_all.38 = bf16[4,8,128,128]{3,2,1,0:T(8,128)(2,1)S(1)} all-to-all(bf16[4,8,128,128]{3,2,1,0:T(8,128)(2,1)S(1)} %broadcast_in_dim.5), channel_id=1, replica_groups={{0,2,8,10},{4,6,12,14},{16,18,24,26},{20,22,28,30},{32,34,40,42},{36,38..., dimensions={0} | all-to-all | bytes 2097152 | tf_op jit(solution)/shard_map/all_to_all | solution.py:85
  102.1 0.8 collective-permute-start.2
  102.9 2.3 %collective-permute-done.2.refs_1_ = bf16[32,128,128]{2,1,0:T(8,128)(2,1)S(1)} collective-permute-done((bf16[32,128,128]{2,1,0:T(8,128)(2,1)S(1)}, bf16[32,128,128]{2,1,0:T(8,128)(2,1)S(1)}, u32[]{:S(2)}, u32[]{:S(2)}) %collective-permute-start.2) | collective-permute-done | bytes 1048608 | tf_op jit(solution)/shard_map/ppermute | solution.py:40
  105.2 0.0 copy-done
  105.2 2.6 %shard_map.136 = (f32[32,128,128]{2,1,0:T(8,128)S(1)}, bf16[32,128,128]{2,1,0:T(8,128)(2,1)S(1)}, f32[128,128]{1,0:T(8,128)S(1)}) custom-call(bf16[32,128,128]{2,1,0:T(8,128)(2,1)S(1)} %bitcast.11, bf16[32,128,128]{2,1,0:T(8,128)(2,1)S(1)} %collective-permute-done.2.refs_1_, f32[32,128]{1,0:T(8,128)S(1)} %bitcast.15, bf16[4096,256]{1,0:T(8,128)(2,1)S(1)} %copy-done, ...), custom_call_target="tpu_custom_call" | custom-call | tf_op jit(solution)/shard_map/pallas_call | solution.py:26
  107.8 0.5 collective-permute-start.3
  108.3 2.3 %collective-permute-done.3 = bf16[32,128,128]{2,1,0:T(8,128)(2,1)S(1)} collective-permute-done((bf16[32,128,128]{2,1,0:T(8,128)(2,1)S(1)}, bf16[32,128,128]{2,1,0:T(8,128)(2,1)S(1)}, u32[]{:S(2)}, u32[]{:S(2)}) %collective-permute-start.3) | collective-permute-done | bytes 1048608 | tf_op jit(solution)/shard_map/ppermute | solution.py:40
  110.6 0.4 add_convert_fusion
  110.9 12.2 %all_to_all.39 = bf16[4,8,128,128]{3,2,1,0:T(8,128)(2,1)S(1)} all-to-all(bf16[4,8,128,128]{3,2,1,0:T(8,128)(2,1)S(1)} %bitcast.16), channel_id=1, replica_groups={{0,2,8,10},{4,6,12,14},{16,18,24,26},{20,22,28,30},{32,34,40,42},{36,38..., dimensions={0} | all-to-all | bytes 2097152 | tf_op jit(solution)/shard_map/all_to_all | solution.py:85
  123.1 0.2 reduce_sum.25
  123.3 16.8 %all_to_all.40.parts = bf16[8,128,128]{2,1,0:T(8,128)(2,1)S(1)} all-to-all(bf16[8,128,128]{2,1,0:T(8,128)(2,1)S(1)} %reduce_sum.25), channel_id=1, replica_groups={{0,4,16,20,32,36,48,52},{2,6,18,22,34,38,50,54},{8,12,24,28,40,44,56,60..., dimensions={0} | all-to-all | bytes 524288 | tf_op jit(solution)/shard_map/all_to_all | solution.py:85
  140.1 0.7 shard_map.137
  (9 shorter events, 0.0 us)
Async XLA Ops:
  0.6 1.5 %collective-permute-start = (bf16[64,256]{1,0:T(8,128)(2,1)}, bf16[64,256]{1,0:T(8,128)(2,1)S(1)}, u32[]{:S(2)}, u32[]{:S(2)}) collective-permute-start(bf16[64,256]{1,0:T(8,128)(2,1)} %bitcast.18), channel_id=1, source_target_pairs={{0,1},{1,0},{2,3},{3,2},{4,5},{5,4},{6,7},{7,6},{8,9},{9,8},{10,11... | collective-permute-start | bytes 98312 | tf_op jit(solution)/shard_map/ppermute | solution.py:40
  20.6 10.2 %copy-start.5 = (f32[16]{0:T(128)S(1)}, f32[16]{0:T(128)}, u32[]{:S(2)}) copy-start(f32[16]{0:T(128)} %param.15) | copy-start | bytes 196
  21.7 24.2 %all-to-all-start.1 = ((bf16[8,8,3200]{2,1,0:T(8,128)(2,1)}), bf16[8,8,3200]{2,1,0:T(8,128)(2,1)S(1)}, u32[]{:S(2)}, u32[]{:S(2)}) async-start(bf16[8,8,3200]{2,1,0:T(8,128)(2,1)} %reduce_sum.24), calls=%async_computation.1 | async-start | bytes 819200 | tf_op jit(solution)/shard_map/all_to_all | solution.py:85
  31.0 1.6 %copy-start.2 = (f32[8,8,64,128]{3,2,1,0:T(8,128)S(1)}, f32[8,8,64,128]{3,2,1,0:T(8,128)}, u32[]{:S(2)}) copy-start(f32[8,8,64,128]{3,2,1,0:T(8,128)} %param.23) | copy-start | bytes 6291460
  32.8 38.8 %copy-start.3 = (bf16[1024,128]{1,0:T(8,128)(2,1)S(1)}, bf16[1024,128]{1,0:T(8,128)(2,1)}, u32[]{:S(2)}) copy-start(bf16[1024,128]{1,0:T(8,128)(2,1)} %w_mix.1) | copy-start | bytes 786436
  71.9 1.3 collective-permute-start.1
  73.2 32.0 %copy-start = (bf16[4096,256]{1,0:T(8,128)(2,1)S(1)}, bf16[4096,256]{1,0:T(8,128)(2,1)}, u32[]{:S(2)}) copy-start(bf16[4096,256]{1,0:T(8,128)(2,1)} %refs_3_.3) | copy-start | bytes 6291460
  73.2 32.0 %copy-start.1 = (bf16[256,4096]{1,0:T(8,128)(2,1)S(1)}, bf16[256,4096]{1,0:T(8,128)(2,1)}, u32[]{:S(2)}) copy-start(bf16[256,4096]{1,0:T(8,128)(2,1)} %refs_4_.3) | copy-start | bytes 6291460
  73.2 32.0 %copy-start.4 = (f32[4096]{0:T(1024)S(1)}, f32[4096]{0:T(1024)}, u32[]{:S(2)}) copy-start(f32[4096]{0:T(1024)} %param.14) | copy-start | bytes 49156
  102.1 3.1 %collective-permute-start.2 = (bf16[32,128,128]{2,1,0:T(8,128)(2,1)S(1)}, bf16[32,128,128]{2,1,0:T(8,128)(2,1)S(1)}, u32[]{:S(2)}, u32[]{:S(2)}) collective-permute-start(bf16[32,128,128]{2,1,0:T(8,128)(2,1)S(1)} %bitcast.10), channel_id=1, source_target_pairs={{0,1},{1,0},{2,3},{3,2},{4,5},{5,4},{6,7},{7,6},{8,9},{9,8},{10,11... | collective-permute-start | bytes 3145736 | tf_op jit(solution)/shard_map/ppermute | solution.py:40
  107.8 2.8 %collective-permute-start.3 = (bf16[32,128,128]{2,1,0:T(8,128)(2,1)S(1)}, bf16[32,128,128]{2,1,0:T(8,128)(2,1)S(1)}, u32[]{:S(2)}, u32[]{:S(2)}) collective-permute-start(bf16[32,128,128]{2,1,0:T(8,128)(2,1)S(1)} %get-tuple-element.17), channel_id=1, source_target_pairs={{0,1},{1,0},{2,3},{3,2},{4,5},{5,4},{6,7},{7,6},{8,9},{9,8},{10,11... | collective-permute-start | bytes 3145736 | tf_op jit(solution)/shard_map/ppermute | solution.py:40

commit v4 on v3

--- a/solution.py
+++ b/solution.py
@@ -44,68 +44,70 @@
     return lax.axis_size("kv_0"), lax.axis_size("kv_1")
 
 
-def parity_order(z_size, x_size):
+def own_class():
+    return 2 * (lax.axis_index("kv_0") % 2) + lax.axis_index("kv_1") % 2
+
+
+def members(z_size, x_size):
+    return [(zr, xr) for zr in range(z_size // 2) for xr in range(x_size // 2)]
+
+
+def member_kv(member, which, x_size):
+    return (2 * member[0] + which // 2) * x_size + 2 * member[1] + which % 2
+
+
+def class_groups():
+    z_size, x_size = ring_sizes()
     return [
-        (2 * zr + zb) * x_size + 2 * xr + xb
-        for zb in range(2)
-        for xb in range(2)
-        for zr in range(z_size // 2)
-        for xr in range(x_size // 2)
-    ]
-
-
-def square_groups(z_size, x_size):
-    groups = []
-    for tp in range(2):
-        for zs in range(z_size // 2):
-            for xs in range(x_size // 2):
-                at_z = {z % 2: z for z in ((2 * zs + tp + i) % z_size for i in range(2))}
-                at_x = {x % 2: x for x in ((2 * xs + tp + i) % x_size for i in range(2))}
-                groups.append(
-                    [
-                        (at_z[zb] * x_size + at_x[xb]) * 2 + tp
-                        for zb in range(2)
-                        for xb in range(2)
-                    ]
-                )
-    return groups
-
-
-def parity_groups(z_size, x_size):
-    order = parity_order(z_size, x_size)
-    count = len(order) // 4
-    return [
-        [kv * 2 + tp for kv in order[c * count : (c + 1) * count]]
+        [member_kv(m, c, x_size) * 2 + tp for m in members(z_size, x_size)]
         for tp in range(2)
         for c in range(4)
     ]
 
 
-def in_groups(x, groups):
-    return lax.all_to_all(x, KV_TP, 0, 0, axis_index_groups=groups, tiled=True)
+def to_neighbour(x, place):
+    z_size, x_size = ring_sizes()
+
+    def across(position, tp, size):
+        return (position + (1 if position % 2 == tp else -1)) % size
+
+    pairs = []
+    for z in range(z_size):
+        for x_ in range(x_size):
+            for tp in range(2):
+                to_z = across(z, tp, z_size) if place & 2 else z
+                to_x = across(x_, tp, x_size) if place & 1 else x_
+                pairs.append(((z * x_size + x_) * 2 + tp, (to_z * x_size + to_x) * 2 + tp))
+    return lax.ppermute(x, KV_TP, pairs)
+
+
+def in_class(x):
+    return lax.all_to_all(x, KV_TP, 0, 0, axis_index_groups=class_groups(), tiled=True)
+
+
+PLACES = (3, 1, 2)
 
 
 def sum_at_owner(parts):
-    sizes = ring_sizes()
-    peers, *rest = parts.shape
-    near = in_groups(parts.reshape(4, peers // 4, *rest), square_groups(*sizes))
-    total = near.reshape(4, peers // 4, *rest).astype(F32).sum(axis=0).astype(BF16)
-    return in_groups(total, parity_groups(*sizes))
+    arrived = {place: to_neighbour(parts[place], place) for place in PLACES}
+    total = parts[0].astype(F32)
+    for place in PLACES:
+        total = total + arrived[place].astype(F32)
+    return in_class(total.astype(BF16))
 
 
 def gathered(copies):
-    sizes = ring_sizes()
-    count, *rest = copies.shape
-    far = in_groups(copies, parity_groups(*sizes))
-    near = in_groups(jnp.broadcast_to(far[None], (4, count, *rest)), square_groups(*sizes))
-    return near.reshape(4 * count, *rest)
+    far = in_class(copies)
+    arrived = {place: to_neighbour(far, place) for place in PLACES}
+    return [far, *(arrived[place] for place in (1, 2, 3))]
 
 
 def inputs_kernel(
-    other, own, gain, w_query, w_key, w_value, w_gate, out, both_out, *scratch, order
+    other, own, gain, w_query, w_key, w_value, w_gate, *rest, sizes
 ):
+    outs, both_out, scratch = rest[:4], rest[4], rest[5:]
     sources = (own, gain, w_query, w_key, w_value, w_gate)
-    held, sem = scratch[:-1], scratch[-1]
+    held, by_class, sem = scratch[:-2], scratch[-2], scratch[-1]
     copies = [
         pltpu.make_async_copy(source, dest, sem.at[i])
         for i, (source, dest) in enumerate(zip(sources, held, strict=True))
@@ -122,8 +124,11 @@
         jnp.concatenate([second, first], axis=0),
     ).T
     both_out[...] = both.astype(BF16)
-    seqs = both.shape[0] // len(order)
-    both = jnp.concatenate([both[i * seqs : (i + 1) * seqs] for i in order], axis=0)
+    seqs = both.shape[0] // (sizes[0] * sizes[1])
+    for c in range(4):
+        kvs = [member_kv(m, c, sizes[1]) for m in members(*sizes)]
+        by_class[c] = jnp.concatenate([both[i * seqs : (i + 1) * seqs] for i in kvs], axis=0)
+    both = jnp.concatenate([by_class[own_class() ^ place] for place in range(4)], axis=0)
     squares = jnp.sum(both * both, axis=1, keepdims=True)
     high = squares.astype(BF16).astype(F32)
     low = squares - high
@@ -134,11 +139,15 @@
     for weight, copy in zip(held[2:], copies[2:], strict=True):
         copy.wait()
         width = weight.shape[1]
-        out[:, start : start + width] = dot(scaled, weight[...]).astype(BF16)
+        product = dot(scaled, weight[...]).astype(BF16)
+        for place, out in enumerate(outs):
+            count = out.shape[0]
+            out[:, start : start + width] = product[place * count : (place + 1) * count]
         start += width
-    out[:, start : start + LANES] = jnp.where(
-        lane == 0, high, jnp.where(lane == 1, low, 0.0)
-    ).astype(BF16)
+    totals = jnp.where(lane == 0, high, jnp.where(lane == 1, low, 0.0)).astype(BF16)
+    for place, out in enumerate(outs):
+        count = out.shape[0]
+        out[:, start : start + LANES] = totals[place * count : (place + 1) * count]
 
 
 def decay_kernel(state, rates, out):
@@ -189,13 +198,20 @@
             heads_out[j, :, cols] = done
 
 
-def mix_kernel(heads, w_mix, keep, send):
+def mix_kernel(*refs, sizes):
+    heads, w_mix, keep, send, product = refs[:4], *refs[4:]
     tp = lax.axis_index("tp")
+    seqs = heads[0].shape[0] // len(members(*sizes))
+    for place in range(4):
+        piece = dot(heads[place][...], w_mix[...])
+        for i, m in enumerate(members(*sizes)):
+            kv = member_kv(m, own_class() ^ place, sizes[1])
+            product[pl.ds(pl.multiple_of(kv * seqs, seqs), seqs), :] = piece[
+                i * seqs : (i + 1) * seqs
+            ]
     half = keep.shape[0]
-    product = dot(heads[...], w_mix[...]).astype(BF16)
-    top, bottom = product[:half], product[half:]
-    keep[...] = jnp.where(tp == 0, top.astype(F32), bottom.astype(F32)).astype(BF16)
-    send[...] = jnp.where(tp == 0, bottom.astype(F32), top.astype(F32)).astype(BF16)
+    keep[...] = product[pl.ds(pl.multiple_of(tp * half, half), half), :].astype(BF16)
+    send[...] = product[pl.ds(pl.multiple_of((1 - tp) * half, half), half), :].astype(BF16)
 
 
 def resid_kernel(both, keep, received, out):
@@ -207,43 +223,56 @@
         out[j] = resid
 
 
-def mixer_kernel(mine, other, gain, w_up, w_down, keep, send, resid, *, model_width, order):
+def mixer_kernel(*refs, model_width, sizes):
+    mine, other, (gain, w_up, w_down), refs = refs[:4], refs[4:8], refs[8:11], refs[11:]
+    keep, send, resid = refs[:4], refs[4:8], refs[8]
     tp = lax.axis_index("tp")
-    kv = lax.axis_index(KV)
-    peers, half, width = mine.shape
+    kv_own = lax.axis_index(KV)
+    count, half, width = mine[0].shape
     hidden_width = w_up.shape[1]
     lane = lax.broadcasted_iota(jnp.int32, (half, width), 1)
     own = jnp.where(lane < width // 2, 0, 1) == tp
     squares = jnp.zeros((2 * half, width), F32)
     upper = jnp.zeros((2 * half, hidden_width), F32)
-    own_resid = jnp.zeros((half, width), F32)
-    for j in range(0, peers, 2):
-        pieces = []
-        for i in (j, j + 1):
-            block = jnp.concatenate([mine[i], other[i]], axis=0).astype(F32)
-            squares = squares + block * block
-            pieces.append((block * gain[order[i] : order[i] + 1, :]).astype(BF16))
-            place = jnp.where(kv == order[i], 1, 0)
-            resid_here = jnp.where(
-                own, block[:half], pltpu.roll(block[half:], width // 2, 1)
+
+    def kv_at(place, i):
+        return member_kv(members(*sizes)[i], own_class() ^ place, sizes[1])
+
+    for place in range(4):
+        for j in range(0, count, 2):
+            pieces, weights = [], []
+            for i in (j, j + 1):
+                kv = kv_at(place, i)
+                block = jnp.concatenate([mine[place][i], other[place][i]], axis=0).astype(F32)
+                squares = squares + block * block
+                pieces.append((block * gain[pl.ds(kv, 1), :]).astype(BF16))
+                weights.append(w_up[pl.ds(pl.multiple_of(kv * width, width), width), :])
+            upper = upper + dot(
+                jnp.concatenate(pieces, axis=1), jnp.concatenate(weights, axis=0)
             )
-            own_resid = jnp.where(place == 1, resid_here, own_resid)
-        weights = [w_up[order[i] * width : (order[i] + 1) * width, :] for i in (j, j + 1)]
-        upper = upper + dot(
-            jnp.concatenate(pieces, axis=1), jnp.concatenate(weights, axis=0)
-        )
-    resid[...] = own_resid
+    spot = (kv_own // sizes[1] // 2) * (sizes[1] // 2) + kv_own % sizes[1] // 2
+    resid[...] = jnp.where(
+        own,
+        mine[0][spot].astype(F32),
+        pltpu.roll(other[0][spot].astype(F32), width // 2, 1),
+    )
     scale = lax.rsqrt(jnp.sum(squares, axis=1, keepdims=True) / model_width + EPS)
     upper = jnp.maximum(upper * scale, 0.0)
     hidden = (upper * upper).astype(BF16)
-    for j in range(0, peers, 2):
-        weights = [w_down[:, order[i] * width : (order[i] + 1) * width] for i in (j, j + 1)]
-        pair = dot(hidden, jnp.concatenate(weights, axis=1))
-        for i in (j, j + 1):
-            cols = slice((i - j) * width, (i - j + 1) * width)
-            from_mine, from_other = pair[:half, cols], pair[half:, cols]
-            keep[i] = jnp.where(own, from_mine, pltpu.roll(from_other, width // 2, 1))
-            send[i] = jnp.where(own, pltpu.roll(from_mine, width // 2, 1), from_other).astype(BF16)
+    for place in (3, 1, 2, 0):
+        for j in range(0, count, 2):
+            weights = [
+                w_down[:, pl.ds(pl.multiple_of(kv_at(place, i) * width, width), width)]
+                for i in (j, j + 1)
+            ]
+            pair = dot(hidden, jnp.concatenate(weights, axis=1))
+            for i in (j, j + 1):
+                cols = slice((i - j) * width, (i - j + 1) * width)
+                from_mine, from_other = pair[:half, cols], pair[half:, cols]
+                keep[place][i] = jnp.where(own, from_mine, pltpu.roll(from_other, width // 2, 1))
+                send[place][i] = jnp.where(
+                    own, pltpu.roll(from_mine, width // 2, 1), from_other
+                ).astype(BF16)
 
 
 def result_kernel(parts, resid, out):
@@ -276,29 +305,32 @@
     cols = 2 * own_cols
     peers = lax.axis_size(KV)
     model_width = cols * peers
-    order = parity_order(*ring_sizes())
+    sizes = ring_sizes()
+    count = peers // 4
     qkvg = sum(w.shape[1] for w in (w_query, w_key, w_value, w_gate))
+    payload_width = qkvg + LANES
     tokens_t = tokens.T
 
     def inputs_body(*refs):
-        inputs_kernel(*refs, order=order)
+        inputs_kernel(*refs, sizes=sizes)
 
     sources = [
         pltpu.with_memory_space_constraint(x, pltpu.HBM)
         for x in (tokens_t, gain_mix.reshape(peers, cols), w_query, w_key, w_value, w_gate)
     ]
-    payload, both = kernel_call(
+    *payload, both = kernel_call(
         inputs_body,
-        [((rows, qkvg + LANES), BF16), ((rows, cols), BF16)],
+        [((rows // 4, payload_width), BF16)] * 4 + [((rows, cols), BF16)],
         swap_tp(tokens_t),
         *sources,
         hbm=range(1, 7),
         scratch=[
             *(pltpu.VMEM(s.shape, s.dtype) for s in sources),
+            pltpu.VMEM((4, rows // 4, cols), F32),
             pltpu.SemaphoreType.DMA((len(sources),)),
         ],
     )
-    parts = sum_at_owner(payload.reshape(peers, seqs, qkvg + LANES))
+    parts = sum_at_owner([piece.reshape(count, seqs, payload_width) for piece in payload])
     rates = lax.dynamic_slice_in_dim(decay_rate, lax.axis_index("tp") * heads, heads)
     (decayed,) = kernel_call(
         decay_kernel,
@@ -318,38 +350,45 @@
         retention_body,
         [
             ((seqs * heads, key_width, value_width), F32),
-            ((peers, seqs, heads * value_width), BF16),
+            ((count, seqs, heads * value_width), BF16),
         ],
         parts,
         decayed,
         scratch=[pltpu.VMEM((seqs, heads * value_width), F32)],
     )
-    all_heads = lax.all_to_all(heads_out, KV, 0, 0, tiled=True)
+
+    def mix_body(*refs):
+        mix_kernel(*refs, sizes=sizes)
+
     keep, send = kernel_call(
-        mix_kernel,
+        mix_body,
         [((half, cols), BF16)] * 2,
-        all_heads.reshape(rows, heads * value_width),
+        *(x.reshape(rows // 4, heads * value_width) for x in gathered(heads_out)),
         w_mix,
+        scratch=[pltpu.VMEM((rows, cols), F32)],
     )
     (resid,) = kernel_call(
-        resid_kernel, [((peers // 4, half, cols), BF16)], both, keep, swap_tp(send)
+        resid_kernel, [((count, half, cols), BF16)], both, keep, swap_tp(send)
     )
     mine = gathered(resid)
-    other = swap_tp(mine)
+    other = [swap_tp(x) for x in mine]
 
     def mixer_body(*refs):
-        mixer_kernel(*refs, model_width=model_width, order=order)
-
-    keep, send, own_resid = kernel_call(
+        mixer_kernel(*refs, model_width=model_width, sizes=sizes)
+
+    piece = (count, half, cols)
+    *out, own_resid = kernel_call(
         mixer_body,
-        [((peers, half, cols), F32), ((peers, half, cols), BF16), ((half, cols), F32)],
-        mine,
-        other,
+        [(piece, F32)] * 4 + [(piece, BF16)] * 4 + [((half, cols), F32)],
+        *mine,
+        *other,
         gain_mlp.reshape(peers, cols),
         w_up,
         w_down,
     )
-    chip_sum = (keep + swap_tp(send).astype(F32)).astype(BF16)
+    chip_sum = {}
+    for place in (*PLACES, 0):
+        chip_sum[place] = (out[place] + swap_tp(out[4 + place]).astype(F32)).astype(BF16)
     parts = sum_at_owner(chip_sum)
     (result_t,) = kernel_call(result_kernel, [((own_cols, rows), BF16)], parts, own_resid)
     return (result_t.T, new_state.reshape(state.shape))

time: 144 us -> 130 us (0.903); the launches traced: 141 us -> 129 us
  blocking collectives: 97.2 us -> 47.3 us
  waiting for transfers between devices: 20.4 us -> 43.1 us
  starting transfers between devices: 10.6 us -> 26.3 us
    all_to_all x6 -> x3, blocking collectives: 97.2 us -> 47.3 us  [in_class(): lax.all_to_all(x, KV_TP, 0, 0, axis_index_groups=class_groups(), tiled=True)]
    ppermute x0 -> x12, waiting for transfers between devices: none -> 27.1 us  [to_neighbour(): return lax.ppermute(x, KV_TP, pairs)]
    ppermute x0 -> x12, starting transfers between devices: none -> 14.3 us  [to_neighbour(): return lax.ppermute(x, KV_TP, pairs)]
    ppermute x4 -> x10, waiting for transfers between devices: 7.17 us -> 4.51 us  [swap_tp(): return lax.ppermute(x, 'tp', [(0, 1), (1, 0)])]
    all_to_all x1, waiting for transfers between devices: 13.2 us -> 11.6 us  [in_class(): lax.all_to_all(x, KV_TP, 0, 0, axis_index_groups=class_groups(), tiled=True)]
  transfers between devices with their start and end apart: 5 -> 23, of which waited for: 5 -> 16; matrix products, arithmetic and copies ran while one was open for 0% -> 0% of each run, Pallas kernels for 0% -> 0%
where the time goes in v4:
time: 130 us; the launch traced here: 129 us
  blocking collectives  47.3 us (36%)
  waiting for transfers between devices  43.1 us (33%)
  starting transfers between devices  26.3 us (20%)
  Pallas kernels  8.32 us (6%)
  local copies, waits for them, and re-layouts  1.76 us (1%)
    all_to_all x3, blocking collectives, in_class(): lax.all_to_all(x, KV_TP, 0, 0, axis_index_groups=class_groups(), tiled=True)  47.3 us
    ppermute x12, waiting for transfers between devices, to_neighbour(): return lax.ppermute(x, KV_TP, pairs)  27.1 us
    ppermute x12, starting transfers between devices, to_neighbour(): return lax.ppermute(x, KV_TP, pairs)  14.3 us
    all_to_all x1, waiting for transfers between devices, in_class(): lax.all_to_all(x, KV_TP, 0, 0, axis_index_groups=class_groups(), tiled=True)  11.6 us
    all_to_all x1, starting transfers between devices, in_class(): lax.all_to_all(x, KV_TP, 0, 0, axis_index_groups=class_groups(), tiled=True)  10 us
    pallas_call x7, Pallas kernels, kernel_call(): pl.pallas_call(body, out_shape=[jax.ShapeDtypeStruct(*o) for o in outs],...  8.32 us
    ppermute x10, waiting for transfers between devices, swap_tp(): return lax.ppermute(x, 'tp', [(0, 1), (1, 0)])  4.51 us
  transfers between devices with their start and end apart: 23, of which 16 were waited for; matrix products, arithmetic and copies ran while one was open for 0% of the time, Pallas kernels for 0%

profile of v4, /device:TPU:18, one launch (start us, length us, event | category | flops | bytes accessed | tf_op | source)
XLA Modules:
  0.0 128.8 jit_solution(7606544046028338680)
XLA Ops:
  0.7 1.4 %collective-permute-done.refs_0_ = bf16[64,256]{1,0:T(8,128)(2,1)S(1)} collective-permute-done((bf16[64,256]{1,0:T(8,128)(2,1)}, bf16[64,256]{1,0:T(8,128)(2,1)S(1)}, u32[]{:S(2)}, u32[]{:S(2)}) %collective-permute-start) | collective-permute-done | bytes 32800 | tf_op jit(solution)/shard_map/ppermute | solution.py:40
  2.1 2.1 %shard_map.131 = (bf16[64,3200]{1,0:T(8,128)(2,1)S(1)}, bf16[64,3200]{1,0:T(8,128)(2,1)S(1)}, bf16[64,3200]{1,0:T(8,128)(2,1)S(1)}, bf16[64,3200]{1,0:T(8,128)(2,1)S(1)}, bf16[256,128]{1,0:T(8,128)(2,1)S(1)}) custom-call(bf16[64,256]{1,0:T(8,128)(2,1)S(1)} %collective-permute-done.refs_0_, bf16[64,256]{1,0:T(8,128)(2,1)} %bitcast.27, f32[32,128]{1,0:T(8,128)} %bitcast.28, ...), custom_call_target="tpu_custom_call" | custom-call | tf_op jit(solution)/shard_map/pallas_call | solution.py:26
  4.2 2.0 %collective-permute-start.1 = (bf16[8,8,3200]{2,1,0:T(8,128)(2,1)S(1)}, bf16[8,8,3200]{2,1,0:T(8,128)(2,1)S(1)}, u32[]{:S(2)}, u32[]{:S(2)}) collective-permute-start(bf16[8,8,3200]{2,1,0:T(8,128)(2,1)S(1)} %bitcast.24), channel_id=1, source_target_pairs={{0,10},{1,63},{2,8},{3,61},{4,14},{5,59},{6,12},{7,57},{8,2},{9,23... | collective-permute-start | bytes 1228808 | tf_op jit(solution)/shard_map/ppermute | solution.py:81
  6.2 1.5 %collective-permute-start.2 = (bf16[8,8,3200]{2,1,0:T(8,128)(2,1)S(1)}, bf16[8,8,3200]{2,1,0:T(8,128)(2,1)S(1)}, u32[]{:S(2)}, u32[]{:S(2)}) collective-permute-start(bf16[8,8,3200]{2,1,0:T(8,128)(2,1)S(1)} %bitcast.23), channel_id=1, source_target_pairs={{0,2},{1,7},{2,0},{3,5},{4,6},{5,3},{6,4},{7,1},{8,10},{9,15},{10,... | collective-permute-start | bytes 1228808 | tf_op jit(solution)/shard_map/ppermute | solution.py:81
  7.8 5.5 %collective-permute-done.1 = bf16[8,8,3200]{2,1,0:T(8,128)(2,1)S(1)} collective-permute-done((bf16[8,8,3200]{2,1,0:T(8,128)(2,1)S(1)}, bf16[8,8,3200]{2,1,0:T(8,128)(2,1)S(1)}, u32[]{:S(2)}, u32[]{:S(2)}) %collective-permute-start.1) | collective-permute-done | bytes 409632 | tf_op jit(solution)/shard_map/ppermute | solution.py:81
  13.3 4.3 %collective-permute-done.2 = bf16[8,8,3200]{2,1,0:T(8,128)(2,1)S(1)} collective-permute-done((bf16[8,8,3200]{2,1,0:T(8,128)(2,1)S(1)}, bf16[8,8,3200]{2,1,0:T(8,128)(2,1)S(1)}, u32[]{:S(2)}, u32[]{:S(2)}) %collective-permute-start.2) | collective-permute-done | bytes 409632 | tf_op jit(solution)/shard_map/ppermute | solution.py:81
  17.6 1.0 fusion.2
  18.5 10.0 %all-to-all-start = ((bf16[8,8,3200]{2,1,0:T(8,128)(2,1)}), bf16[8,8,3200]{2,1,0:T(8,128)(2,1)S(1)}, u32[]{:S(2)}, u32[]{:S(2)}) async-start(bf16[8,8,3200]{2,1,0:T(8,128)(2,1)} %fusion.2), calls=%async_computation | async-start | bytes 819200 | tf_op jit(solution)/shard_map/all_to_all | solution.py:85
  28.7 1.6 %copy-done.2 = f32[8,8,64,128]{3,2,1,0:T(8,128)S(1)} copy-done((f32[8,8,64,128]{3,2,1,0:T(8,128)S(1)}, f32[8,8,64,128]{3,2,1,0:T(8,128)}, u32[]{:S(2)}) %copy-start.2) | copy-done | bytes 2097176
  30.5 11.6 %all-to-all-done.refs_0_ = bf16[8,8,3200]{2,1,0:T(8,128)(2,1)S(1)} async-done(((bf16[8,8,3200]{2,1,0:T(8,128)(2,1)}), bf16[8,8,3200]{2,1,0:T(8,128)(2,1)S(1)}, u32[]{:S(2)}, u32[]{:S(2)}) %all-to-all-start) | async-done | bytes 409632 | tf_op jit(solution)/shard_map/all_to_all | solution.py:85
  42.0 2.5 %shard_map.133 = (f32[64,64,128]{2,1,0:T(8,128)}, bf16[8,8,1024]{2,1,0:T(8,128)(2,1)S(1)}) custom-call(bf16[8,8,3200]{2,1,0:T(8,128)(2,1)S(1)} %all-to-all-done.refs_0_, f32[64,64,128]{2,1,0:T(8,128)S(1)} %shard_map.132.refs_1_), custom_call_target="tpu_custom_call" | custom-call | tf_op jit(solution)/shard_map/pallas_call | solution.py:26
  44.6 15.4 %all_to_all.20 = bf16[8,8,1024]{2,1,0:T(8,128)(2,1)S(1)} all-to-all(bf16[8,8,1024]{2,1,0:T(8,128)(2,1)S(1)} %get-tuple-element.25), channel_id=1, replica_groups={{0,4,16,20,32,36,48,52},{2,6,18,22,34,38,50,54},{8,12,24,28,40,44,56,60..., dimensions={0} | all-to-all | bytes 262144 | tf_op jit(solution)/shard_map/all_to_all | solution.py:85
  60.4 2.4 %collective-permute-start.5 = (bf16[8,8,1024]{2,1,0:T(8,128)(2,1)S(1)}, bf16[8,8,1024]{2,1,0:T(8,128)(2,1)S(1)}, u32[]{:S(2)}, u32[]{:S(2)}) collective-permute-start(bf16[8,8,1024]{2,1,0:T(8,128)(2,1)S(1)} %all_to_all.20), channel_id=1, source_target_pairs={{0,8},{1,57},{2,10},{3,59},{4,12},{5,61},{6,14},{7,63},{8,0},{9,17... | collective-permute-start | bytes 393224 | tf_op jit(solution)/shard_map/ppermute | solution.py:81
  62.8 0.7 collective-permute-start.4
  63.5 2.4 %collective-permute-done.6 = bf16[8,8,1024]{2,1,0:T(8,128)(2,1)S(1)} collective-permute-done((bf16[8,8,1024]{2,1,0:T(8,128)(2,1)S(1)}, bf16[8,8,1024]{2,1,0:T(8,128)(2,1)S(1)}, u32[]{:S(2)}, u32[]{:S(2)}) %collective-permute-start.6) | collective-permute-done | bytes 131104 | tf_op jit(solution)/shard_map/ppermute | solution.py:81
  65.9 1.3 collective-permute-done.5
  67.2 0.6 collective-permute-done.4
  68.2 1.2 collective-permute-done.7.received
  69.4 14.2 %all_to_all.21.refs_0_ = bf16[8,128,128]{2,1,0:T(8,128)(2,1)S(1)} all-to-all(bf16[8,128,128]{2,1,0:T(8,128)(2,1)S(1)} %shard_map.135), channel_id=1, replica_groups={{0,4,16,20,32,36,48,52},{2,6,18,22,34,38,50,54},{8,12,24,28,40,44,56,60..., dimensions={0} | all-to-all | bytes 524288 | tf_op jit(solution)/shard_map/all_to_all | solution.py:85
  83.7 1.1 collective-permute-start.10
  84.7 2.0 %collective-permute-start.9 = (bf16[8,128,128]{2,1,0:T(8,128)(2,1)S(1)}, bf16[8,128,128]{2,1,0:T(8,128)(2,1)S(1)}, u32[]{:S(2)}, u32[]{:S(2)}) collective-permute-start(bf16[8,128,128]{2,1,0:T(8,128)(2,1)S(1)} %all_to_all.21.refs_0_), channel_id=1, source_target_pairs={{0,8},{1,57},{2,10},{3,59},{4,12},{5,61},{6,14},{7,63},{8,0},{9,17... | collective-permute-start | bytes 786440 | tf_op jit(solution)/shard_map/ppermute | solution.py:81
  87.3 3.7 %collective-permute-done.10.refs_3_ = bf16[8,128,128]{2,1,0:T(8,128)(2,1)S(1)} collective-permute-done((bf16[8,128,128]{2,1,0:T(8,128)(2,1)S(1)}, bf16[8,128,128]{2,1,0:T(8,128)(2,1)S(1)}, u32[]{:S(2)}, u32[]{:S(2)}) %collective-permute-start.10) | collective-permute-done | bytes 262176 | tf_op jit(solution)/shard_map/ppermute | solution.py:81
  91.0 2.9 %collective-permute-done.9.refs_2_ = bf16[8,128,128]{2,1,0:T(8,128)(2,1)S(1)} collective-permute-done((bf16[8,128,128]{2,1,0:T(8,128)(2,1)S(1)}, bf16[8,128,128]{2,1,0:T(8,128)(2,1)S(1)}, u32[]{:S(2)}, u32[]{:S(2)}) %collective-permute-start.9) | collective-permute-done | bytes 262176 | tf_op jit(solution)/shard_map/ppermute | solution.py:81
  94.4 1.0 collective-permute-done.13.refs_6_
  95.8 2.5 %shard_map.136 = (f32[8,128,128]{2,1,0:T(8,128)S(1)}, f32[8,128,128]{2,1,0:T(8,128)S(1)}, f32[8,128,128]{2,1,0:T(8,128)S(1)}, f32[8,128,128]{2,1,0:T(8,128)S(1)}...) custom-call(bf16[8,128,128]{2,1,0:T(8,128)(2,1)S(1)} %all_to_all.21., ...), custom_call_target="tpu_custom_call" | custom-call | tf_op jit(solution)/shard_map/pallas_call | solution.py:26
  100.0 1.2 collective-permute-start.17
  101.3 0.7 collective-permute-start.19
  102.1 1.8 %collective-permute-start.21 = (bf16[8,128,128]{2,1,0:T(8,128)(2,1)S(1)}, bf16[8,128,128]{2,1,0:T(8,128)(2,1)S(1)}, u32[]{:S(2)}, u32[]{:S(2)}) collective-permute-start(bf16[8,128,128]{2,1,0:T(8,128)(2,1)S(1)} %add_convert_fusion.1), channel_id=1, source_target_pairs={{0,8},{1,57},{2,10},{3,59},{4,12},{5,61},{6,14},{7,63},{8,0},{9,17... | collective-permute-start | bytes 786440 | tf_op jit(solution)/shard_map/ppermute | solution.py:81
  103.9 3.6 %collective-permute-done.17 = bf16[8,128,128]{2,1,0:T(8,128)(2,1)S(1)} collective-permute-done((bf16[8,128,128]{2,1,0:T(8,128)(2,1)S(1)}, bf16[8,128,128]{2,1,0:T(8,128)(2,1)S(1)}, u32[]{:S(2)}, u32[]{:S(2)}) %collective-permute-start.17) | collective-permute-done | bytes 262176 | tf_op jit(solution)/shard_map/ppermute | solution.py:81
  107.5 2.7 %collective-permute-done.19 = bf16[8,128,128]{2,1,0:T(8,128)(2,1)S(1)} collective-permute-done((bf16[8,128,128]{2,1,0:T(8,128)(2,1)S(1)}, bf16[8,128,128]{2,1,0:T(8,128)(2,1)S(1)}, u32[]{:S(2)}, u32[]{:S(2)}) %collective-permute-start.19) | collective-permute-done | bytes 262176 | tf_op jit(solution)/shard_map/ppermute | solution.py:81
  110.4 17.6 %all_to_all.22.parts = bf16[8,128,128]{2,1,0:T(8,128)(2,1)S(1)} all-to-all(bf16[8,128,128]{2,1,0:T(8,128)(2,1)S(1)} %add_convert_fusion), channel_id=1, replica_groups={{0,4,16,20,32,36,48,52},{2,6,18,22,34,38,50,54},{8,12,24,28,40,44,56,60..., dimensions={0} | all-to-all | bytes 524288 | tf_op jit(solution)/shard_map/all_to_all | solution.py:85
  128.1 0.7 shard_map.137
  (43 shorter events, 4.9 us)
Async XLA Ops:
  0.6 27.9 %copy-start.5 = (f32[16]{0:T(128)S(1)}, f32[16]{0:T(128)}, u32[]{:S(2)}) copy-start(f32[16]{0:T(128)} %param.15) | copy-start | bytes 196
  0.6 1.5 %collective-permute-start = (bf16[64,256]{1,0:T(8,128)(2,1)}, bf16[64,256]{1,0:T(8,128)(2,1)S(1)}, u32[]{:S(2)}, u32[]{:S(2)}) collective-permute-start(bf16[64,256]{1,0:T(8,128)(2,1)} %bitcast.26), channel_id=1, source_target_pairs={{0,1},{1,0},{2,3},{3,2},{4,5},{5,4},{6,7},{7,6},{8,9},{9,8},{10,11... | collective-permute-start | bytes 98312 | tf_op jit(solution)/shard_map/ppermute | solution.py:40
  4.2 9.0 %collective-permute-start.1 = (bf16[8,8,3200]{2,1,0:T(8,128)(2,1)S(1)}, bf16[8,8,3200]{2,1,0:T(8,128)(2,1)S(1)}, u32[]{:S(2)}, u32[]{:S(2)}) collective-permute-start(bf16[8,8,3200]{2,1,0:T(8,128)(2,1)S(1)} %bitcast.24), channel_id=1, source_target_pairs={{0,10},{1,63},{2,8},{3,61},{4,14},{5,59},{6,12},{7,57},{8,2},{9,23... | collective-permute-start | bytes 1228808 | tf_op jit(solution)/shard_map/ppermute | solution.py:81
  6.2 11.4 %collective-permute-start.2 = (bf16[8,8,3200]{2,1,0:T(8,128)(2,1)S(1)}, bf16[8,8,3200]{2,1,0:T(8,128)(2,1)S(1)}, u32[]{:S(2)}, u32[]{:S(2)}) collective-permute-start(bf16[8,8,3200]{2,1,0:T(8,128)(2,1)S(1)} %bitcast.23), channel_id=1, source_target_pairs={{0,2},{1,7},{2,0},{3,5},{4,6},{5,3},{6,4},{7,1},{8,10},{9,15},{10,... | collective-permute-start | bytes 1228808 | tf_op jit(solution)/shard_map/ppermute | solution.py:81
  7.7 9.9 %collective-permute-start.3 = (bf16[8,8,3200]{2,1,0:T(8,128)(2,1)S(1)}, bf16[8,8,3200]{2,1,0:T(8,128)(2,1)S(1)}, u32[]{:S(2)}, u32[]{:S(2)}) collective-permute-start(bf16[8,8,3200]{2,1,0:T(8,128)(2,1)S(1)} %bitcast.22), channel_id=1, source_target_pairs={{0,8},{1,57},{2,10},{3,59},{4,12},{5,61},{6,14},{7,63},{8,0},{9,17... | collective-permute-start | bytes 1228808 | tf_op jit(solution)/shard_map/ppermute | solution.py:81
  18.5 23.5 %all-to-all-start = ((bf16[8,8,3200]{2,1,0:T(8,128)(2,1)}), bf16[8,8,3200]{2,1,0:T(8,128)(2,1)S(1)}, u32[]{:S(2)}, u32[]{:S(2)}) async-start(bf16[8,8,3200]{2,1,0:T(8,128)(2,1)} %fusion.2), calls=%async_computation | async-start | bytes 819200 | tf_op jit(solution)/shard_map/all_to_all | solution.py:85
  28.7 1.6 %copy-start.2 = (f32[8,8,64,128]{3,2,1,0:T(8,128)S(1)}, f32[8,8,64,128]{3,2,1,0:T(8,128)}, u32[]{:S(2)}) copy-start(f32[8,8,64,128]{3,2,1,0:T(8,128)} %param.23) | copy-start | bytes 6291460
  30.5 37.3 %copy-start.3 = (bf16[1024,128]{1,0:T(8,128)(2,1)S(1)}, bf16[1024,128]{1,0:T(8,128)(2,1)}, u32[]{:S(2)}) copy-start(bf16[1024,128]{1,0:T(8,128)(2,1)} %refs_4_.3) | copy-start | bytes 786436
  30.5 65.4 %copy-start.4 = (f32[4096]{0:T(1024)S(1)}, f32[4096]{0:T(1024)}, u32[]{:S(2)}) copy-start(f32[4096]{0:T(1024)} %param.14) | copy-start | bytes 49156
  42.0 53.8 %copy-start = (bf16[4096,256]{1,0:T(8,128)(2,1)S(1)}, bf16[4096,256]{1,0:T(8,128)(2,1)}, u32[]{:S(2)}) copy-start(bf16[4096,256]{1,0:T(8,128)(2,1)} %refs_9_.1) | copy-start | bytes 6291460
  42.0 53.8 %copy-start.1 = (bf16[256,4096]{1,0:T(8,128)(2,1)S(1)}, bf16[256,4096]{1,0:T(8,128)(2,1)}, u32[]{:S(2)}) copy-start(bf16[256,4096]{1,0:T(8,128)(2,1)} %refs_10_.1) | copy-start | bytes 6291460
  60.0 5.9 %collective-permute-start.6 = (bf16[8,8,1024]{2,1,0:T(8,128)(2,1)S(1)}, bf16[8,8,1024]{2,1,0:T(8,128)(2,1)S(1)}, u32[]{:S(2)}, u32[]{:S(2)}) collective-permute-start(bf16[8,8,1024]{2,1,0:T(8,128)(2,1)S(1)} %all_to_all.20), channel_id=1, source_target_pairs={{0,10},{1,63},{2,8},{3,61},{4,14},{5,59},{6,12},{7,57},{8,2},{9,23... | collective-permute-start | bytes 393224 | tf_op jit(solution)/shard_map/ppermute | solution.py:81
  60.4 6.7 %collective-permute-start.5 = (bf16[8,8,1024]{2,1,0:T(8,128)(2,1)S(1)}, bf16[8,8,1024]{2,1,0:T(8,128)(2,1)S(1)}, u32[]{:S(2)}, u32[]{:S(2)}) collective-permute-start(bf16[8,8,1024]{2,1,0:T(8,128)(2,1)S(1)} %all_to_all.20), channel_id=1, source_target_pairs={{0,8},{1,57},{2,10},{3,59},{4,12},{5,61},{6,14},{7,63},{8,0},{9,17... | collective-permute-start | bytes 393224 | tf_op jit(solution)/shard_map/ppermute | solution.py:81
  62.8 5.0 %collective-permute-start.4 = (bf16[8,8,1024]{2,1,0:T(8,128)(2,1)S(1)}, bf16[8,8,1024]{2,1,0:T(8,128)(2,1)S(1)}, u32[]{:S(2)}, u32[]{:S(2)}) collective-permute-start(bf16[8,8,1024]{2,1,0:T(8,128)(2,1)S(1)} %all_to_all.20), channel_id=1, source_target_pairs={{0,2},{1,7},{2,0},{3,5},{4,6},{5,3},{6,4},{7,1},{8,10},{9,15},{10,... | collective-permute-start | bytes 393224 | tf_op jit(solution)/shard_map/ppermute | solution.py:81
  68.1 1.3 %collective-permute-start.7 = (bf16[128,128]{1,0:T(8,128)(2,1)S(1)}, bf16[128,128]{1,0:T(8,128)(2,1)S(1)}, u32[]{:S(2)}, u32[]{:S(2)}) collective-permute-start(bf16[128,128]{1,0:T(8,128)(2,1)S(1)} %get-tuple-element.27), channel_id=1, source_target_pairs={{0,1},{1,0},{2,3},{3,2},{4,5},{5,4},{6,7},{7,6},{8,9},{9,8},{10,11... | collective-permute-start | bytes 98312 | tf_op jit(solution)/shard_map/ppermute | solution.py:40
  83.7 7.3 %collective-permute-start.10 = (bf16[8,128,128]{2,1,0:T(8,128)(2,1)S(1)}, bf16[8,128,128]{2,1,0:T(8,128)(2,1)S(1)}, u32[]{:S(2)}, u32[]{:S(2)}) collective-permute-start(bf16[8,128,128]{2,1,0:T(8,128)(2,1)S(1)} %all_to_all.21.refs_0_), channel_id=1, source_target_pairs={{0,10},{1,63},{2,8},{3,61},{4,14},{5,59},{6,12},{7,57},{8,2},{9,23... | collective-permute-start | bytes 786440 | tf_op jit(solution)/shard_map/ppermute | solution.py:81
  84.7 9.2 %collective-permute-start.9 = (bf16[8,128,128]{2,1,0:T(8,128)(2,1)S(1)}, bf16[8,128,128]{2,1,0:T(8,128)(2,1)S(1)}, u32[]{:S(2)}, u32[]{:S(2)}) collective-permute-start(bf16[8,128,128]{2,1,0:T(8,128)(2,1)S(1)} %all_to_all.21.refs_0_), channel_id=1, source_target_pairs={{0,8},{1,57},{2,10},{3,59},{4,12},{5,61},{6,14},{7,63},{8,0},{9,17... | collective-permute-start | bytes 786440 | tf_op jit(solution)/shard_map/ppermute | solution.py:81
  86.7 7.2 %collective-permute-start.8 = (bf16[8,128,128]{2,1,0:T(8,128)(2,1)S(1)}, bf16[8,128,128]{2,1,0:T(8,128)(2,1)S(1)}, u32[]{:S(2)}, u32[]{:S(2)}) collective-permute-start(bf16[8,128,128]{2,1,0:T(8,128)(2,1)S(1)} %all_to_all.21.refs_0_), channel_id=1, source_target_pairs={{0,2},{1,7},{2,0},{3,5},{4,6},{5,3},{6,4},{7,1},{8,10},{9,15},{10,... | collective-permute-start | bytes 786440 | tf_op jit(solution)/shard_map/ppermute | solution.py:81
  87.1 7.3 %collective-permute-start.11 = (bf16[8,128,128]{2,1,0:T(8,128)(2,1)S(1)}, bf16[8,128,128]{2,1,0:T(8,128)(2,1)S(1)}, u32[]{:S(2)}, u32[]{:S(2)}) collective-permute-start(bf16[8,128,128]{2,1,0:T(8,128)(2,1)S(1)} %all_to_all.21.refs_0_), channel_id=1, source_target_pairs={{0,1},{1,0},{2,3},{3,2},{4,5},{5,4},{6,7},{7,6},{8,9},{9,8},{10,11... | collective-permute-start | bytes 786440 | tf_op jit(solution)/shard_map/ppermute | solution.py:40
  91.0 3.4 %collective-permute-start.14 = (bf16[8,128,128]{2,1,0:T(8,128)(2,1)S(1)}, bf16[8,128,128]{2,1,0:T(8,128)(2,1)S(1)}, u32[]{:S(2)}, u32[]{:S(2)}) collective-permute-start(bf16[8,128,128]{2,1,0:T(8,128)(2,1)S(1)} %collective-permute-done.10.refs_3_), channel_id=1, source_target_pairs={{0,1},{1,0},{2,3},{3,2},{4,5},{5,4},{6,7},{7,6},{8,9},{9,8},{10,11... | collective-permute-start | bytes 786440 | tf_op jit(solution)/shard_map/ppermute | solution.py:40
  93.9 1.5 %collective-permute-start.13 = (bf16[8,128,128]{2,1,0:T(8,128)(2,1)S(1)}, bf16[8,128,128]{2,1,0:T(8,128)(2,1)S(1)}, u32[]{:S(2)}, u32[]{:S(2)}) collective-permute-start(bf16[8,128,128]{2,1,0:T(8,128)(2,1)S(1)} %collective-permute-done.9.refs_2_), channel_id=1, source_target_pairs={{0,1},{1,0},{2,3},{3,2},{4,5},{5,4},{6,7},{7,6},{8,9},{9,8},{10,11... | collective-permute-start | bytes 786440 | tf_op jit(solution)/shard_map/ppermute | solution.py:40
  93.9 1.9 %collective-permute-start.12 = (bf16[8,128,128]{2,1,0:T(8,128)(2,1)S(1)}, bf16[8,128,128]{2,1,0:T(8,128)(2,1)S(1)}, u32[]{:S(2)}, u32[]{:S(2)}) collective-permute-start(bf16[8,128,128]{2,1,0:T(8,128)(2,1)S(1)} %collective-permute-done.8.refs_1_), channel_id=1, source_target_pairs={{0,1},{1,0},{2,3},{3,2},{4,5},{5,4},{6,7},{7,6},{8,9},{9,8},{10,11... | collective-permute-start | bytes 786440 | tf_op jit(solution)/shard_map/ppermute | solution.py:40
  98.3 1.6 %collective-permute-start.16 = (bf16[8,128,128]{2,1,0:T(8,128)(2,1)S(1)}, bf16[8,128,128]{2,1,0:T(8,128)(2,1)S(1)}, u32[]{:S(2)}, u32[]{:S(2)}) collective-permute-start(bf16[8,128,128]{2,1,0:T(8,128)(2,1)S(1)} %get-tuple-element.31), channel_id=1, source_target_pairs={{0,1},{1,0},{2,3},{3,2},{4,5},{5,4},{6,7},{7,6},{8,9},{9,8},{10,11... | collective-permute-start | bytes 786440 | tf_op jit(solution)/shard_map/ppermute | solution.py:40
  98.6 2.7 %collective-permute-start.18 = (bf16[8,128,128]{2,1,0:T(8,128)(2,1)S(1)}, bf16[8,128,128]{2,1,0:T(8,128)(2,1)S(1)}, u32[]{:S(2)}, u32[]{:S(2)}) collective-permute-start(bf16[8,128,128]{2,1,0:T(8,128)(2,1)S(1)} %get-tuple-element.33), channel_id=1, source_target_pairs={{0,1},{1,0},{2,3},{3,2},{4,5},{5,4},{6,7},{7,6},{8,9},{9,8},{10,11... | collective-permute-start | bytes 786440 | tf_op jit(solution)/shard_map/ppermute | solution.py:40
  98.9 5.0 %collective-permute-start.15 = (bf16[8,128,128]{2,1,0:T(8,128)(2,1)S(1)}, bf16[8,128,128]{2,1,0:T(8,128)(2,1)S(1)}, u32[]{:S(2)}, u32[]{:S(2)}) collective-permute-start(bf16[8,128,128]{2,1,0:T(8,128)(2,1)S(1)} %get-tuple-element.29), channel_id=1, source_target_pairs={{0,1},{1,0},{2,3},{3,2},{4,5},{5,4},{6,7},{7,6},{8,9},{9,8},{10,11... | collective-permute-start | bytes 786440 | tf_op jit(solution)/shard_map/ppermute | solution.py:40
  99.1 2.9 %collective-permute-start.20 = (bf16[8,128,128]{2,1,0:T(8,128)(2,1)S(1)}, bf16[8,128,128]{2,1,0:T(8,128)(2,1)S(1)}, u32[]{:S(2)}, u32[]{:S(2)}) collective-permute-start(bf16[8,128,128]{2,1,0:T(8,128)(2,1)S(1)} %get-tuple-element.35), channel_id=1, source_target_pairs={{0,1},{1,0},{2,3},{3,2},{4,5},{5,4},{6,7},{7,6},{8,9},{9,8},{10,11... | collective-permute-start | bytes 786440 | tf_op jit(solution)/shard_map/ppermute | solution.py:40
  100.0 7.5 %collective-permute-start.17 = (bf16[8,128,128]{2,1,0:T(8,128)(2,1)S(1)}, bf16[8,128,128]{2,1,0:T(8,128)(2,1)S(1)}, u32[]{:S(2)}, u32[]{:S(2)}) collective-permute-start(bf16[8,128,128]{2,1,0:T(8,128)(2,1)S(1)} %add_convert_fusion.3), channel_id=1, source_target_pairs={{0,10},{1,63},{2,8},{3,61},{4,14},{5,59},{6,12},{7,57},{8,2},{9,23... | collective-permute-start | bytes 786440 | tf_op jit(solution)/shard_map/ppermute | solution.py:81
  101.3 8.9 %collective-permute-start.19 = (bf16[8,128,128]{2,1,0:T(8,128)(2,1)S(1)}, bf16[8,128,128]{2,1,0:T(8,128)(2,1)S(1)}, u32[]{:S(2)}, u32[]{:S(2)}) collective-permute-start(bf16[8,128,128]{2,1,0:T(8,128)(2,1)S(1)} %add_convert_fusion.2), channel_id=1, source_target_pairs={{0,2},{1,7},{2,0},{3,5},{4,6},{5,3},{6,4},{7,1},{8,10},{9,15},{10,... | collective-permute-start | bytes 786440 | tf_op jit(solution)/shard_map/ppermute | solution.py:81
  102.1 8.2 %collective-permute-start.21 = (bf16[8,128,128]{2,1,0:T(8,128)(2,1)S(1)}, bf16[8,128,128]{2,1,0:T(8,128)(2,1)S(1)}, u32[]{:S(2)}, u32[]{:S(2)}) collective-permute-start(bf16[8,128,128]{2,1,0:T(8,128)(2,1)S(1)} %add_convert_fusion.1), channel_id=1, source_target_pairs={{0,8},{1,57},{2,10},{3,59},{4,12},{5,61},{6,14},{7,63},{8,0},{9,17... | collective-permute-start | bytes 786440 | tf_op jit(solution)/shard_map/ppermute | solution.py:81

commit v5 on v4

--- a/solution.py
+++ b/solution.py
@@ -29,7 +29,7 @@
         in_specs=[in_hbm if i in hbm else vmem for i in range(len(args))],
         out_specs=[vmem] * len(outs),
         scratch_shapes=list(scratch),
-        compiler_params=pltpu.CompilerParams(vmem_limit_bytes=20 * 2**20),
+        compiler_params=pltpu.CompilerParams(vmem_limit_bytes=10 * 2**20),
         cost_estimate=pl.CostEstimate(
             flops=flops, bytes_accessed=bytes_accessed, transcendentals=0
         ),
@@ -88,36 +88,36 @@
 PLACES = (3, 1, 2)
 
 
-def sum_at_owner(parts):
+def sum_in_square(parts):
     arrived = {place: to_neighbour(parts[place], place) for place in PLACES}
     total = parts[0].astype(F32)
     for place in PLACES:
         total = total + arrived[place].astype(F32)
-    return in_class(total.astype(BF16))
-
-
-def gathered(copies):
-    far = in_class(copies)
-    arrived = {place: to_neighbour(far, place) for place in PLACES}
-    return [far, *(arrived[place] for place in (1, 2, 3))]
-
-
-def inputs_kernel(
-    other, own, gain, w_query, w_key, w_value, w_gate, *rest, sizes
-):
-    outs, both_out, scratch = rest[:4], rest[4], rest[5:]
-    sources = (own, gain, w_query, w_key, w_value, w_gate)
-    held, by_class, sem = scratch[:-2], scratch[-2], scratch[-1]
+    return total.astype(BF16)
+
+
+def from_square(own):
+    arrived = {place: to_neighbour(own, place) for place in PLACES}
+    return [own, *(arrived[place] for place in (1, 2, 3))]
+
+
+def fetch_kernel(*refs):
+    count = len(refs) // 2
+    sem = refs[-1]
     copies = [
-        pltpu.make_async_copy(source, dest, sem.at[i])
-        for i, (source, dest) in enumerate(zip(sources, held, strict=True))
+        pltpu.make_async_copy(refs[i], refs[count + i], sem.at[i]) for i in range(count)
     ]
     for copy in copies:
         copy.start()
+    for copy in copies:
+        copy.wait()
+
+
+def inputs_kernel(other, own, gain, w_query, w_key, w_value, w_gate, *rest, sizes):
+    outs, both_out, by_class = rest[:4], rest[4], rest[5]
     tp = lax.axis_index("tp")
     kv = lax.axis_index(KV)
-    copies[0].wait()
-    first, second = held[0][...].astype(F32), other[...].astype(F32)
+    first, second = own[...].astype(F32), other[...].astype(F32)
     both = jnp.where(
         tp == 0,
         jnp.concatenate([first, second], axis=0),
@@ -133,11 +133,9 @@
     high = squares.astype(BF16).astype(F32)
     low = squares - high
     lane = lax.broadcasted_iota(jnp.int32, (squares.shape[0], LANES), 1)
-    copies[1].wait()
-    scaled = (both * held[1][pl.ds(kv, 1), :]).astype(BF16)
+    scaled = (both * gain[pl.ds(kv, 1), :]).astype(BF16)
     start = 0
-    for weight, copy in zip(held[2:], copies[2:], strict=True):
-        copy.wait()
+    for weight in (w_query, w_key, w_value, w_gate):
         width = weight.shape[1]
         product = dot(scaled, weight[...]).astype(BF16)
         for place, out in enumerate(outs):
@@ -158,7 +156,9 @@
         out[i] = decay[h : h + 1, :] * state[i]
 
 
-def retention_kernel(parts, decayed, new_state, heads_out, read_ref, *, model_width, sizes):
+def retention_kernel(
+    parts, decayed, heads_out, key_out, value_out, read_ref, *, model_width, sizes
+):
     seqs, heads, key_width, value_width = sizes
     total = parts[0].astype(F32)
     for j in range(1, parts.shape[0]):
@@ -178,24 +178,38 @@
     value = rounded(total[:, k_end:v_end])
     gate = rounded(total[:, v_end:g_end])
     query_t = query.T
-    key_t = key.T
+    key_out[...] = key.T
+    value_out[...] = value
     for b in range(seqs):
         for h in range(heads):
             rows = slice(h * key_width, (h + 1) * key_width)
             cols = slice(h * value_width, (h + 1) * value_width)
-            new = decayed[b * heads + h] + key_t[rows, b : b + 1] * value[b : b + 1, cols]
-            new_state[b * heads + h] = new
             read_ref[b : b + 1, cols] = jnp.sum(
-                query_t[rows, b : b + 1] * new, axis=0, keepdims=True
+                query_t[rows, b : b + 1] * decayed[b * heads + h], axis=0, keepdims=True
             )
     for h in range(heads):
+        rows = slice(h * key_width, (h + 1) * key_width)
         cols = slice(h * value_width, (h + 1) * value_width)
-        read = read_ref[:, cols]
+        match = jnp.sum(query[:, rows] * key[:, rows], axis=1, keepdims=True)
+        read = read_ref[:, cols] + match * value[:, cols]
         read = read * lax.rsqrt(jnp.mean(read * read, axis=1, keepdims=True) + EPS)
         g = gate[:, cols]
         done = (g / (1.0 + jnp.exp(-g)) * read).astype(BF16)
         for j in range(heads_out.shape[0]):
             heads_out[j, :, cols] = done
+
+
+def state_kernel(decayed, key_t, value, new_state):
+    seqs, width = value.shape
+    key_width, value_width = decayed.shape[1:]
+    heads = width // value_width
+    for b in range(seqs):
+        for h in range(heads):
+            rows = slice(h * key_width, (h + 1) * key_width)
+            cols = slice(h * value_width, (h + 1) * value_width)
+            new_state[b * heads + h] = (
+                decayed[b * heads + h] + key_t[rows, b : b + 1] * value[b : b + 1, cols]
+            )
 
 
 def mix_kernel(*refs, sizes):
@@ -223,56 +237,61 @@
         out[j] = resid
 
 
-def mixer_kernel(*refs, model_width, sizes):
-    mine, other, (gain, w_up, w_down), refs = refs[:4], refs[4:8], refs[8:11], refs[11:]
-    keep, send, resid = refs[:4], refs[4:8], refs[8]
-    tp = lax.axis_index("tp")
-    kv_own = lax.axis_index(KV)
-    count, half, width = mine[0].shape
-    hidden_width = w_up.shape[1]
-    lane = lax.broadcasted_iota(jnp.int32, (half, width), 1)
-    own = jnp.where(lane < width // 2, 0, 1) == tp
-    squares = jnp.zeros((2 * half, width), F32)
-    upper = jnp.zeros((2 * half, hidden_width), F32)
-
-    def kv_at(place, i):
-        return member_kv(members(*sizes)[i], own_class() ^ place, sizes[1])
-
-    for place in range(4):
-        for j in range(0, count, 2):
-            pieces, weights = [], []
-            for i in (j, j + 1):
-                kv = kv_at(place, i)
-                block = jnp.concatenate([mine[place][i], other[place][i]], axis=0).astype(F32)
-                squares = squares + block * block
-                pieces.append((block * gain[pl.ds(kv, 1), :]).astype(BF16))
-                weights.append(w_up[pl.ds(pl.multiple_of(kv * width, width), width), :])
-            upper = upper + dot(
-                jnp.concatenate(pieces, axis=1), jnp.concatenate(weights, axis=0)
-            )
-    spot = (kv_own // sizes[1] // 2) * (sizes[1] // 2) + kv_own % sizes[1] // 2
-    resid[...] = jnp.where(
-        own,
-        mine[0][spot].astype(F32),
-        pltpu.roll(other[0][spot].astype(F32), width // 2, 1),
-    )
+def up_kernel(mine, other, gain, w_up, upper, squares, *, place, sizes):
+    count, half, width = mine.shape
+    total = jnp.zeros((2 * half, w_up.shape[1]), F32)
+    square = jnp.zeros((2 * half, width), F32)
+    for j in range(0, count, 2):
+        pieces, weights = [], []
+        for i in (j, j + 1):
+            kv = member_kv(members(*sizes)[i], own_class() ^ place, sizes[1])
+            block = jnp.concatenate([mine[i], other[i]], axis=0).astype(F32)
+            square = square + block * block
+            pieces.append((block * gain[pl.ds(kv, 1), :]).astype(BF16))
+            weights.append(w_up[pl.ds(pl.multiple_of(kv * width, width), width), :])
+        total = total + dot(jnp.concatenate(pieces, axis=1), jnp.concatenate(weights, axis=0))
+    upper[...] = total
+    squares[...] = square
+
+
+def hidden_of(refs, model_width):
+    upper = sum(ref[...] for ref in refs[0::2])
+    squares = sum(ref[...] for ref in refs[1::2])
     scale = lax.rsqrt(jnp.sum(squares, axis=1, keepdims=True) / model_width + EPS)
     upper = jnp.maximum(upper * scale, 0.0)
-    hidden = (upper * upper).astype(BF16)
-    for place in (3, 1, 2, 0):
-        for j in range(0, count, 2):
-            weights = [
-                w_down[:, pl.ds(pl.multiple_of(kv_at(place, i) * width, width), width)]
-                for i in (j, j + 1)
-            ]
-            pair = dot(hidden, jnp.concatenate(weights, axis=1))
-            for i in (j, j + 1):
-                cols = slice((i - j) * width, (i - j + 1) * width)
-                from_mine, from_other = pair[:half, cols], pair[half:, cols]
-                keep[place][i] = jnp.where(own, from_mine, pltpu.roll(from_other, width // 2, 1))
-                send[place][i] = jnp.where(
-                    own, pltpu.roll(from_mine, width // 2, 1), from_other
-                ).astype(BF16)
+    return (upper * upper).astype(BF16)
+
+
+def own_lanes(half, width):
+    lane = lax.broadcasted_iota(jnp.int32, (half, width), 1)
+    return jnp.where(lane < width // 2, 0, 1) == lax.axis_index("tp")
+
+
+def down_kernel(hidden, w_down, keep, send, *, place, sizes):
+    count, half, width = keep.shape
+    own = own_lanes(half, width)
+    for j in range(0, count, 2):
+        weights = []
+        for i in (j, j + 1):
+            kv = member_kv(members(*sizes)[i], own_class() ^ place, sizes[1])
+            weights.append(w_down[:, pl.ds(pl.multiple_of(kv * width, width), width)])
+        pair = dot(hidden[...], jnp.concatenate(weights, axis=1))
+        for i in (j, j + 1):
+            cols = slice((i - j) * width, (i - j + 1) * width)
+            from_mine, from_other = pair[:half, cols], pair[half:, cols]
+            keep[i] = jnp.where(own, from_mine, pltpu.roll(from_other, width // 2, 1))
+            send[i] = jnp.where(own, pltpu.roll(from_mine, width // 2, 1), from_other).astype(BF16)
+
+
+def own_resid_kernel(mine, other, resid, *, sizes):
+    half, width = resid.shape
+    kv = lax.axis_index(KV)
+    spot = (kv // sizes[1] // 2) * (sizes[1] // 2) + kv % sizes[1] // 2
+    resid[...] = jnp.where(
+        own_lanes(half, width),
+        mine[spot].astype(F32),
+        pltpu.roll(other[spot].astype(F32), width // 2, 1),
+    )
 
 
 def result_kernel(parts, resid, out):
@@ -318,44 +337,62 @@
         pltpu.with_memory_space_constraint(x, pltpu.HBM)
         for x in (tokens_t, gain_mix.reshape(peers, cols), w_query, w_key, w_value, w_gate)
     ]
+    fetched = kernel_call(
+        fetch_kernel,
+        [(x.shape, x.dtype) for x in sources],
+        *sources,
+        hbm=range(len(sources)),
+        scratch=[pltpu.SemaphoreType.DMA((len(sources),))],
+        flops=10**7,
+        bytes_accessed=2**21,
+    )
     *payload, both = kernel_call(
         inputs_body,
         [((rows // 4, payload_width), BF16)] * 4 + [((rows, cols), BF16)],
         swap_tp(tokens_t),
-        *sources,
-        hbm=range(1, 7),
-        scratch=[
-            *(pltpu.VMEM(s.shape, s.dtype) for s in sources),
-            pltpu.VMEM((4, rows // 4, cols), F32),
-            pltpu.SemaphoreType.DMA((len(sources),)),
-        ],
-    )
-    parts = sum_at_owner([piece.reshape(count, seqs, payload_width) for piece in payload])
+        *fetched,
+        scratch=[pltpu.VMEM((4, rows // 4, cols), F32)],
+    )
     rates = lax.dynamic_slice_in_dim(decay_rate, lax.axis_index("tp") * heads, heads)
     (decayed,) = kernel_call(
         decay_kernel,
         [((seqs * heads, key_width, value_width), F32)],
         state.reshape(seqs * heads, key_width, value_width),
         jnp.broadcast_to(rates[:, None], (heads, value_width)),
-        flops=10**7,
+        flops=3 * 10**7,
         bytes_accessed=2**23,
     )
+    total = sum_in_square([piece.reshape(count, seqs, payload_width) for piece in payload])
+    total, decayed = lax.optimization_barrier((total, decayed))
+    parts = in_class(total)
 
     def retention_body(*refs):
         retention_kernel(
             *refs, model_width=model_width, sizes=(seqs, heads, key_width, value_width)
         )
 
-    new_state, heads_out = kernel_call(
+    heads_out, key_t, value = kernel_call(
         retention_body,
         [
-            ((seqs * heads, key_width, value_width), F32),
             ((count, seqs, heads * value_width), BF16),
+            ((heads * key_width, seqs), F32),
+            ((seqs, heads * value_width), F32),
         ],
         parts,
         decayed,
         scratch=[pltpu.VMEM((seqs, heads * value_width), F32)],
     )
+    far_heads = in_class(heads_out)
+    key_t, far_heads = lax.optimization_barrier((key_t, far_heads))
+    (new_state,) = kernel_call(
+        state_kernel,
+        [((seqs * heads, key_width, value_width), F32)],
+        decayed,
+        key_t,
+        value,
+        flops=3 * 10**7,
+        bytes_accessed=2**23,
+    )
 
     def mix_body(*refs):
         mix_kernel(*refs, sizes=sizes)
@@ -363,33 +400,66 @@
     keep, send = kernel_call(
         mix_body,
         [((half, cols), BF16)] * 2,
-        *(x.reshape(rows // 4, heads * value_width) for x in gathered(heads_out)),
+        *(x.reshape(rows // 4, heads * value_width) for x in from_square(far_heads)),
         w_mix,
         scratch=[pltpu.VMEM((rows, cols), F32)],
     )
     (resid,) = kernel_call(
         resid_kernel, [((count, half, cols), BF16)], both, keep, swap_tp(send)
     )
-    mine = gathered(resid)
+    mine = from_square(in_class(resid))
     other = [swap_tp(x) for x in mine]
-
-    def mixer_body(*refs):
-        mixer_kernel(*refs, model_width=model_width, sizes=sizes)
-
+    gains = gain_mlp.reshape(peers, cols)
+    ups = []
+    for place in range(4):
+
+        def up_body(*refs, place=place):
+            up_kernel(*refs, place=place, sizes=sizes)
+
+        ups += kernel_call(
+            up_body,
+            [((rows, w_up.shape[1]), F32), ((rows, cols), F32)],
+            mine[place],
+            other[place],
+            gains,
+            w_up,
+            flops=10**7,
+            bytes_accessed=2**21,
+        )
+
+    def resid_body(*refs):
+        own_resid_kernel(*refs, sizes=sizes)
+
+    (own_resid,) = kernel_call(
+        resid_body, [((half, cols), F32)], mine[0], other[0], flops=10**5
+    )
     piece = (count, half, cols)
-    *out, own_resid = kernel_call(
-        mixer_body,
-        [(piece, F32)] * 4 + [(piece, BF16)] * 4 + [((half, cols), F32)],
-        *mine,
-        *other,
-        gain_mlp.reshape(peers, cols),
-        w_up,
-        w_down,
-    )
     chip_sum = {}
+    hidden = None
     for place in (*PLACES, 0):
-        chip_sum[place] = (out[place] + swap_tp(out[4 + place]).astype(F32)).astype(BF16)
-    parts = sum_at_owner(chip_sum)
+
+        def down_body(*refs, place=place):
+            down_kernel(*refs, place=place, sizes=sizes)
+
+        def first_down_body(*refs, place=place):
+            hidden_ref = refs[-1]
+            hidden_ref[...] = hidden_of(refs[: len(ups)], model_width)
+            down_kernel(hidden_ref, *refs[len(ups) : -1], place=place, sizes=sizes)
+
+        outs = [(piece, F32), (piece, BF16)]
+        if hidden is None:
+            keep, send, hidden = kernel_call(
+                first_down_body, [*outs, ((rows, w_up.shape[1]), BF16)], *ups, w_down
+            )
+        else:
+            keep, send = kernel_call(
+                down_body, outs, hidden, w_down, flops=10**7, bytes_accessed=2**21
+            )
+        chip_sum[place] = (keep + swap_tp(send).astype(F32)).astype(BF16)
+    total, own_resid, new_state = lax.optimization_barrier(
+        (sum_in_square(chip_sum), own_resid, new_state)
+    )
+    parts = in_class(total)
     (result_t,) = kernel_call(result_kernel, [((own_cols, rows), BF16)], parts, own_resid)
     return (result_t.T, new_state.reshape(state.shape))
 

time: 130 us -> 128 us (0.985); the launches traced: 129 us -> 125 us
  blocking collectives: 47.3 us -> 71.3 us
  waiting for transfers between devices: 43.1 us -> 23.8 us
  starting transfers between devices: 26.3 us -> 16.5 us
    all_to_all x3 -> x4, blocking collectives: 47.3 us -> 71.3 us  [in_class(): lax.all_to_all(x, KV_TP, 0, 0, axis_index_groups=class_groups(), tiled=True)]
    all_to_all x1 -> x0, waiting for transfers between devices: 11.6 us -> none  [in_class(): lax.all_to_all(x, KV_TP, 0, 0, axis_index_groups=class_groups(), tiled=True)]
    all_to_all x1 -> x0, starting transfers between devices: 10 us -> none  [in_class(): lax.all_to_all(x, KV_TP, 0, 0, axis_index_groups=class_groups(), tiled=True)]
    ppermute x12, waiting for transfers between devices: 27.1 us -> 22.1 us  [to_neighbour(): return lax.ppermute(x, KV_TP, pairs)]
    ppermute x10, waiting for transfers between devices: 4.51 us -> 1.69 us  [swap_tp(): return lax.ppermute(x, 'tp', [(0, 1), (1, 0)])]
    pallas_call x7 -> x17, Pallas kernels: 8.32 us -> 9.45 us  [kernel_call(): pl.pallas_call(body, out_shape=[jax.ShapeDtypeStruct(*o) for o in outs],...]
  transfers between devices with their start and end apart: 23 -> 22, of which waited for: 16 -> 12; matrix products, arithmetic and copies ran while one was open for 0% -> 1% of each run, Pallas kernels for 0% -> 5%
where the time goes in v5:
time: 128 us; the launch traced here: 125 us
  blocking collectives  71.3 us (56%)
  waiting for transfers between devices  23.8 us (19%)
  starting transfers between devices  16.5 us (13%)
  Pallas kernels  9.45 us (7%)
  local copies, waits for them, and re-layouts  2.98 us (2%)
    all_to_all x4, blocking collectives, in_class(): lax.all_to_all(x, KV_TP, 0, 0, axis_index_groups=class_groups(), tiled=True)  71.3 us
    ppermute x12, waiting for transfers between devices, to_neighbour(): return lax.ppermute(x, KV_TP, pairs)  22.1 us
    ppermute x12, starting transfers between devices, to_neighbour(): return lax.ppermute(x, KV_TP, pairs)  14.3 us
    pallas_call x17, Pallas kernels, kernel_call(): pl.pallas_call(body, out_shape=[jax.ShapeDtypeStruct(*o) for o in outs],...  9.45 us
  transfers between devices with their start and end apart: 22, of which 12 were waited for; matrix products, arithmetic and copies ran while one was open for 1% of the time, Pallas kernels for 5%

profile of v5, /device:TPU:18, one launch (start us, length us, event | category | flops | bytes accessed | tf_op | source)
XLA Modules:
  0.0 125.4 jit_solution(8847065393238280626)
XLA Ops:
  0.7 1.2 shard_map.131
  2.1 0.7 shard_map.132
  2.8 2.0 %collective-permute-start.1 = (bf16[8,8,3200]{2,1,0:T(8,128)(2,1)S(1)}, bf16[8,8,3200]{2,1,0:T(8,128)(2,1)S(1)}, u32[]{:S(2)}, u32[]{:S(2)}) collective-permute-start(bf16[8,8,3200]{2,1,0:T(8,128)(2,1)S(1)} %bitcast.27), channel_id=1, source_target_pairs={{0,10},{1,63},{2,8},{3,61},{4,14},{5,59},{6,12},{7,57},{8,2},{9,23... | collective-permute-start | bytes 1228808 | tf_op jit(solution)/shard_map/ppermute | solution.py:81
  4.8 1.5 %collective-permute-start.2 = (bf16[8,8,3200]{2,1,0:T(8,128)(2,1)S(1)}, bf16[8,8,3200]{2,1,0:T(8,128)(2,1)S(1)}, u32[]{:S(2)}, u32[]{:S(2)}) collective-permute-start(bf16[8,8,3200]{2,1,0:T(8,128)(2,1)S(1)} %bitcast.26), channel_id=1, source_target_pairs={{0,2},{1,7},{2,0},{3,5},{4,6},{5,3},{6,4},{7,1},{8,10},{9,15},{10,... | collective-permute-start | bytes 1228808 | tf_op jit(solution)/shard_map/ppermute | solution.py:81
  6.4 0.7 dynamic_slice.3
  7.2 1.6 %copy-done.2 = f32[8,8,64,128]{3,2,1,0:T(8,128)S(1)} copy-done((f32[8,8,64,128]{3,2,1,0:T(8,128)S(1)}, f32[8,8,64,128]{3,2,1,0:T(8,128)}, u32[]{:S(2)}) %copy-start.2) | copy-done | bytes 2097176
  8.9 2.9 %collective-permute-done.1 = bf16[8,8,3200]{2,1,0:T(8,128)(2,1)S(1)} collective-permute-done((bf16[8,8,3200]{2,1,0:T(8,128)(2,1)S(1)}, bf16[8,8,3200]{2,1,0:T(8,128)(2,1)S(1)}, u32[]{:S(2)}, u32[]{:S(2)}) %collective-permute-start.1) | collective-permute-done | bytes 409632 | tf_op jit(solution)/shard_map/ppermute | solution.py:81
  11.8 4.3 %collective-permute-done.2 = bf16[8,8,3200]{2,1,0:T(8,128)(2,1)S(1)} collective-permute-done((bf16[8,8,3200]{2,1,0:T(8,128)(2,1)S(1)}, bf16[8,8,3200]{2,1,0:T(8,128)(2,1)S(1)}, u32[]{:S(2)}, u32[]{:S(2)}) %collective-permute-start.2) | collective-permute-done | bytes 409632 | tf_op jit(solution)/shard_map/ppermute | solution.py:81
  16.3 24.4 %all_to_all.20.refs_0_ = bf16[8,8,3200]{2,1,0:T(8,128)(2,1)S(1)} all-to-all(bf16[8,8,3200]{2,1,0:T(8,128)(2,1)S(1)} %fusion.2), channel_id=1, replica_groups={{0,4,16,20,32,36,48,52},{2,6,18,22,34,38,50,54},{8,12,24,28,40,44,56,60..., dimensions={0} | all-to-all | bytes 819200 | tf_op jit(solution)/shard_map/all_to_all | solution.py:85
  40.7 0.8 shard_map.134
  41.6 14.8 %all_to_all.21 = bf16[8,8,1024]{2,1,0:T(8,128)(2,1)S(1)} all-to-all(bf16[8,8,1024]{2,1,0:T(8,128)(2,1)S(1)} %get-tuple-element.56), channel_id=1, replica_groups={{0,4,16,20,32,36,48,52},{2,6,18,22,34,38,50,54},{8,12,24,28,40,44,56,60..., dimensions={0} | all-to-all | bytes 262144 | tf_op jit(solution)/shard_map/all_to_all | solution.py:85
  56.4 1.0 collective-permute-start.6
  57.4 1.7 %collective-permute-start.5 = (bf16[8,8,1024]{2,1,0:T(8,128)(2,1)S(1)}, bf16[8,8,1024]{2,1,0:T(8,128)(2,1)S(1)}, u32[]{:S(2)}, u32[]{:S(2)}) collective-permute-start(bf16[8,8,1024]{2,1,0:T(8,128)(2,1)S(1)} %all_to_all.21), channel_id=1, source_target_pairs={{0,8},{1,57},{2,10},{3,59},{4,12},{5,61},{6,14},{7,63},{8,0},{9,17... | collective-permute-start | bytes 393224 | tf_op jit(solution)/shard_map/ppermute | solution.py:81
  59.1 0.8 collective-permute-start.4
  59.9 2.4 %collective-permute-done.6 = bf16[8,8,1024]{2,1,0:T(8,128)(2,1)S(1)} collective-permute-done((bf16[8,8,1024]{2,1,0:T(8,128)(2,1)S(1)}, bf16[8,8,1024]{2,1,0:T(8,128)(2,1)S(1)}, u32[]{:S(2)}, u32[]{:S(2)}) %collective-permute-start.6) | collective-permute-done | bytes 131104 | tf_op jit(solution)/shard_map/ppermute | solution.py:81
  62.3 1.2 collective-permute-done.5
  63.4 0.6 collective-permute-done.4
  64.5 1.2 collective-permute-done.7.received
  65.7 14.2 %all_to_all.22.refs_0_ = bf16[8,128,128]{2,1,0:T(8,128)(2,1)S(1)} all-to-all(bf16[8,128,128]{2,1,0:T(8,128)(2,1)S(1)} %shard_map.136), channel_id=1, replica_groups={{0,4,16,20,32,36,48,52},{2,6,18,22,34,38,50,54},{8,12,24,28,40,44,56,60..., dimensions={0} | all-to-all | bytes 524288 | tf_op jit(solution)/shard_map/all_to_all | solution.py:85
  79.9 1.4 %collective-permute-start.13 = (bf16[8,128,128]{2,1,0:T(8,128)(2,1)S(1)}, bf16[8,128,128]{2,1,0:T(8,128)(2,1)S(1)}, u32[]{:S(2)}, u32[]{:S(2)}) collective-permute-start(bf16[8,128,128]{2,1,0:T(8,128)(2,1)S(1)} %all_to_all.22.refs_0_), channel_id=1, source_target_pairs={{0,10},{1,63},{2,8},{3,61},{4,14},{5,59},{6,12},{7,57},{8,2},{9,23... | collective-permute-start | bytes 786440 | tf_op jit(solution)/shard_map/ppermute | solution.py:81
  81.3 1.5 %collective-permute-start.11 = (bf16[8,128,128]{2,1,0:T(8,128)(2,1)S(1)}, bf16[8,128,128]{2,1,0:T(8,128)(2,1)S(1)}, u32[]{:S(2)}, u32[]{:S(2)}) collective-permute-start(bf16[8,128,128]{2,1,0:T(8,128)(2,1)S(1)} %all_to_all.22.refs_0_), channel_id=1, source_target_pairs={{0,8},{1,57},{2,10},{3,59},{4,12},{5,61},{6,14},{7,63},{8,0},{9,17... | collective-permute-start | bytes 786440 | tf_op jit(solution)/shard_map/ppermute | solution.py:81
  83.5 3.7 %collective-permute-done.13.refs_0_ = bf16[8,128,128]{2,1,0:T(8,128)(2,1)S(1)} collective-permute-done((bf16[8,128,128]{2,1,0:T(8,128)(2,1)S(1)}, bf16[8,128,128]{2,1,0:T(8,128)(2,1)S(1)}, u32[]{:S(2)}, u32[]{:S(2)}) %collective-permute-start.13) | collective-permute-done | bytes 262176 | tf_op jit(solution)/shard_map/ppermute | solution.py:81
  87.3 2.7 %collective-permute-done.11.refs_0_ = bf16[8,128,128]{2,1,0:T(8,128)(2,1)S(1)} collective-permute-done((bf16[8,128,128]{2,1,0:T(8,128)(2,1)S(1)}, bf16[8,128,128]{2,1,0:T(8,128)(2,1)S(1)}, u32[]{:S(2)}, u32[]{:S(2)}) %collective-permute-start.11) | collective-permute-done | bytes 262176 | tf_op jit(solution)/shard_map/ppermute | solution.py:81
  92.8 0.6 shard_map.141
  96.5 2.0 %collective-permute-start.17 = (bf16[8,128,128]{2,1,0:T(8,128)(2,1)S(1)}, bf16[8,128,128]{2,1,0:T(8,128)(2,1)S(1)}, u32[]{:S(2)}, u32[]{:S(2)}) collective-permute-start(bf16[8,128,128]{2,1,0:T(8,128)(2,1)S(1)} %add_convert_fusion.3), channel_id=1, source_target_pairs={{0,10},{1,63},{2,8},{3,61},{4,14},{5,59},{6,12},{7,57},{8,2},{9,23... | collective-permute-start | bytes 786440 | tf_op jit(solution)/shard_map/ppermute | solution.py:81
  98.6 1.0 collective-permute-start.21
  99.7 0.7 collective-permute-start.19
  100.4 1.9 %shard_map.146 = f32[64,64,128]{2,1,0:T(8,128)} custom-call(f32[64,64,128]{2,1,0:T(8,128)S(1)} %shard_map.133.refs_1_.decayed, f32[512,8]{1,0:T(8,128)S(1)} %get-tuple-element.77.key_t, f32[8,1024]{1,0:T(8,128)S(1)} %get-tuple-element.78.value), custom_call_target="tpu_custom_call" | custom-call | flops 30000000 | bytes 8388608 | tf_op jit(solution)/shard_map/pallas_call | solution.py:26
  102.4 1.5 %collective-permute-done.17 = bf16[8,128,128]{2,1,0:T(8,128)(2,1)S(1)} collective-permute-done((bf16[8,128,128]{2,1,0:T(8,128)(2,1)S(1)}, bf16[8,128,128]{2,1,0:T(8,128)(2,1)S(1)}, u32[]{:S(2)}, u32[]{:S(2)}) %collective-permute-start.17) | collective-permute-done | bytes 262176 | tf_op jit(solution)/shard_map/ppermute | solution.py:81
  103.9 2.7 %collective-permute-done.21 = bf16[8,128,128]{2,1,0:T(8,128)(2,1)S(1)} collective-permute-done((bf16[8,128,128]{2,1,0:T(8,128)(2,1)S(1)}, bf16[8,128,128]{2,1,0:T(8,128)(2,1)S(1)}, u32[]{:S(2)}, u32[]{:S(2)}) %collective-permute-start.21) | collective-permute-done | bytes 262176 | tf_op jit(solution)/shard_map/ppermute | solution.py:81
  106.8 17.8 %all_to_all.23.parts = bf16[8,128,128]{2,1,0:T(8,128)(2,1)S(1)} all-to-all(bf16[8,128,128]{2,1,0:T(8,128)(2,1)S(1)} %add_convert_fusion), channel_id=1, replica_groups={{0,4,16,20,32,36,48,52},{2,6,18,22,34,38,50,54},{8,12,24,28,40,44,56,60..., dimensions={0} | all-to-all | bytes 524288 | tf_op jit(solution)/shard_map/all_to_all | solution.py:85
  124.6 0.7 shard_map.147
  (50 shorter events, 8.1 us)
Async XLA Ops:
  0.6 1.5 %collective-permute-start = (bf16[64,256]{1,0:T(8,128)(2,1)}, bf16[64,256]{1,0:T(8,128)(2,1)S(1)}, u32[]{:S(2)}, u32[]{:S(2)}) collective-permute-start(bf16[64,256]{1,0:T(8,128)(2,1)} %bitcast.29), channel_id=1, source_target_pairs={{0,1},{1,0},{2,3},{3,2},{4,5},{5,4},{6,7},{7,6},{8,9},{9,8},{10,11... | collective-permute-start | bytes 98312 | tf_op jit(solution)/shard_map/ppermute | solution.py:40
  2.8 9.0 %collective-permute-start.1 = (bf16[8,8,3200]{2,1,0:T(8,128)(2,1)S(1)}, bf16[8,8,3200]{2,1,0:T(8,128)(2,1)S(1)}, u32[]{:S(2)}, u32[]{:S(2)}) collective-permute-start(bf16[8,8,3200]{2,1,0:T(8,128)(2,1)S(1)} %bitcast.27), channel_id=1, source_target_pairs={{0,10},{1,63},{2,8},{3,61},{4,14},{5,59},{6,12},{7,57},{8,2},{9,23... | collective-permute-start | bytes 1228808 | tf_op jit(solution)/shard_map/ppermute | solution.py:81
  4.8 11.3 %collective-permute-start.2 = (bf16[8,8,3200]{2,1,0:T(8,128)(2,1)S(1)}, bf16[8,8,3200]{2,1,0:T(8,128)(2,1)S(1)}, u32[]{:S(2)}, u32[]{:S(2)}) collective-permute-start(bf16[8,8,3200]{2,1,0:T(8,128)(2,1)S(1)} %bitcast.26), channel_id=1, source_target_pairs={{0,2},{1,7},{2,0},{3,5},{4,6},{5,3},{6,4},{7,1},{8,10},{9,15},{10,... | collective-permute-start | bytes 1228808 | tf_op jit(solution)/shard_map/ppermute | solution.py:81
  6.3 9.9 %collective-permute-start.3 = (bf16[8,8,3200]{2,1,0:T(8,128)(2,1)S(1)}, bf16[8,8,3200]{2,1,0:T(8,128)(2,1)S(1)}, u32[]{:S(2)}, u32[]{:S(2)}) collective-permute-start(bf16[8,8,3200]{2,1,0:T(8,128)(2,1)S(1)} %bitcast.25), channel_id=1, source_target_pairs={{0,8},{1,57},{2,10},{3,59},{4,12},{5,61},{6,14},{7,63},{8,0},{9,17... | collective-permute-start | bytes 1228808 | tf_op jit(solution)/shard_map/ppermute | solution.py:81
  7.2 1.6 %copy-start.2 = (f32[8,8,64,128]{3,2,1,0:T(8,128)S(1)}, f32[8,8,64,128]{3,2,1,0:T(8,128)}, u32[]{:S(2)}) copy-start(f32[8,8,64,128]{3,2,1,0:T(8,128)} %param.23) | copy-start | bytes 6291460
  16.3 47.7 %copy-start.4 = (bf16[1024,128]{1,0:T(8,128)(2,1)S(1)}, bf16[1024,128]{1,0:T(8,128)(2,1)}, u32[]{:S(2)}) copy-start(bf16[1024,128]{1,0:T(8,128)(2,1)} %refs_4_.3) | copy-start | bytes 786436
  40.7 49.8 %copy-start = (bf16[4096,256]{1,0:T(8,128)(2,1)S(1)}, bf16[4096,256]{1,0:T(8,128)(2,1)}, u32[]{:S(2)}) copy-start(bf16[4096,256]{1,0:T(8,128)(2,1)} %refs_3_.9) | copy-start | bytes 6291460
  40.7 49.8 %copy-start.3 = (f32[4096]{0:T(1024)S(1)}, f32[4096]{0:T(1024)}, u32[]{:S(2)}) copy-start(f32[4096]{0:T(1024)} %param.14) | copy-start | bytes 49156
  56.4 5.9 %collective-permute-start.6 = (bf16[8,8,1024]{2,1,0:T(8,128)(2,1)S(1)}, bf16[8,8,1024]{2,1,0:T(8,128)(2,1)S(1)}, u32[]{:S(2)}, u32[]{:S(2)}) collective-permute-start(bf16[8,8,1024]{2,1,0:T(8,128)(2,1)S(1)} %all_to_all.21), channel_id=1, source_target_pairs={{0,10},{1,63},{2,8},{3,61},{4,14},{5,59},{6,12},{7,57},{8,2},{9,23... | collective-permute-start | bytes 393224 | tf_op jit(solution)/shard_map/ppermute | solution.py:81
  57.4 6.0 %collective-permute-start.5 = (bf16[8,8,1024]{2,1,0:T(8,128)(2,1)S(1)}, bf16[8,8,1024]{2,1,0:T(8,128)(2,1)S(1)}, u32[]{:S(2)}, u32[]{:S(2)}) collective-permute-start(bf16[8,8,1024]{2,1,0:T(8,128)(2,1)S(1)} %all_to_all.21), channel_id=1, source_target_pairs={{0,8},{1,57},{2,10},{3,59},{4,12},{5,61},{6,14},{7,63},{8,0},{9,17... | collective-permute-start | bytes 393224 | tf_op jit(solution)/shard_map/ppermute | solution.py:81
  59.1 5.0 %collective-permute-start.4 = (bf16[8,8,1024]{2,1,0:T(8,128)(2,1)S(1)}, bf16[8,8,1024]{2,1,0:T(8,128)(2,1)S(1)}, u32[]{:S(2)}, u32[]{:S(2)}) collective-permute-start(bf16[8,8,1024]{2,1,0:T(8,128)(2,1)S(1)} %all_to_all.21), channel_id=1, source_target_pairs={{0,2},{1,7},{2,0},{3,5},{4,6},{5,3},{6,4},{7,1},{8,10},{9,15},{10,... | collective-permute-start | bytes 393224 | tf_op jit(solution)/shard_map/ppermute | solution.py:81
  64.4 1.3 %collective-permute-start.7 = (bf16[128,128]{1,0:T(8,128)(2,1)S(1)}, bf16[128,128]{1,0:T(8,128)(2,1)S(1)}, u32[]{:S(2)}, u32[]{:S(2)}) collective-permute-start(bf16[128,128]{1,0:T(8,128)(2,1)S(1)} %get-tuple-element.59), channel_id=1, source_target_pairs={{0,1},{1,0},{2,3},{3,2},{4,5},{5,4},{6,7},{7,6},{8,9},{9,8},{10,11... | collective-permute-start | bytes 98312 | tf_op jit(solution)/shard_map/ppermute | solution.py:40
  79.9 7.4 %collective-permute-start.13 = (bf16[8,128,128]{2,1,0:T(8,128)(2,1)S(1)}, bf16[8,128,128]{2,1,0:T(8,128)(2,1)S(1)}, u32[]{:S(2)}, u32[]{:S(2)}) collective-permute-start(bf16[8,128,128]{2,1,0:T(8,128)(2,1)S(1)} %all_to_all.22.refs_0_), channel_id=1, source_target_pairs={{0,10},{1,63},{2,8},{3,61},{4,14},{5,59},{6,12},{7,57},{8,2},{9,23... | collective-permute-start | bytes 786440 | tf_op jit(solution)/shard_map/ppermute | solution.py:81
  81.3 8.7 %collective-permute-start.11 = (bf16[8,128,128]{2,1,0:T(8,128)(2,1)S(1)}, bf16[8,128,128]{2,1,0:T(8,128)(2,1)S(1)}, u32[]{:S(2)}, u32[]{:S(2)}) collective-permute-start(bf16[8,128,128]{2,1,0:T(8,128)(2,1)S(1)} %all_to_all.22.refs_0_), channel_id=1, source_target_pairs={{0,8},{1,57},{2,10},{3,59},{4,12},{5,61},{6,14},{7,63},{8,0},{9,17... | collective-permute-start | bytes 786440 | tf_op jit(solution)/shard_map/ppermute | solution.py:81
  82.8 7.3 %collective-permute-start.9 = (bf16[8,128,128]{2,1,0:T(8,128)(2,1)S(1)}, bf16[8,128,128]{2,1,0:T(8,128)(2,1)S(1)}, u32[]{:S(2)}, u32[]{:S(2)}) collective-permute-start(bf16[8,128,128]{2,1,0:T(8,128)(2,1)S(1)} %all_to_all.22.refs_0_), channel_id=1, source_target_pairs={{0,2},{1,7},{2,0},{3,5},{4,6},{5,3},{6,4},{7,1},{8,10},{9,15},{10,... | collective-permute-start | bytes 786440 | tf_op jit(solution)/shard_map/ppermute | solution.py:81
  83.4 7.1 %collective-permute-start.8 = (bf16[8,128,128]{2,1,0:T(8,128)(2,1)S(1)}, bf16[8,128,128]{2,1,0:T(8,128)(2,1)S(1)}, u32[]{:S(2)}, u32[]{:S(2)}) collective-permute-start(bf16[8,128,128]{2,1,0:T(8,128)(2,1)S(1)} %all_to_all.22.refs_0_), channel_id=1, source_target_pairs={{0,1},{1,0},{2,3},{3,2},{4,5},{5,4},{6,7},{7,6},{8,9},{9,8},{10,11... | collective-permute-start | bytes 786440 | tf_op jit(solution)/shard_map/ppermute | solution.py:40
  87.3 3.6 %collective-permute-start.14 = (bf16[8,128,128]{2,1,0:T(8,128)(2,1)S(1)}, bf16[8,128,128]{2,1,0:T(8,128)(2,1)S(1)}, u32[]{:S(2)}, u32[]{:S(2)}) collective-permute-start(bf16[8,128,128]{2,1,0:T(8,128)(2,1)S(1)} %collective-permute-done.13.refs_0_), channel_id=1, source_target_pairs={{0,1},{1,0},{2,3},{3,2},{4,5},{5,4},{6,7},{7,6},{8,9},{9,8},{10,11... | collective-permute-start | bytes 786440 | tf_op jit(solution)/shard_map/ppermute | solution.py:40
  90.0 1.5 %collective-permute-start.12 = (bf16[8,128,128]{2,1,0:T(8,128)(2,1)S(1)}, bf16[8,128,128]{2,1,0:T(8,128)(2,1)S(1)}, u32[]{:S(2)}, u32[]{:S(2)}) collective-permute-start(bf16[8,128,128]{2,1,0:T(8,128)(2,1)S(1)} %collective-permute-done.11.refs_0_), channel_id=1, source_target_pairs={{0,1},{1,0},{2,3},{3,2},{4,5},{5,4},{6,7},{7,6},{8,9},{9,8},{10,11... | collective-permute-start | bytes 786440 | tf_op jit(solution)/shard_map/ppermute | solution.py:40
  90.1 1.8 %collective-permute-start.10 = (bf16[8,128,128]{2,1,0:T(8,128)(2,1)S(1)}, bf16[8,128,128]{2,1,0:T(8,128)(2,1)S(1)}, u32[]{:S(2)}, u32[]{:S(2)}) collective-permute-start(bf16[8,128,128]{2,1,0:T(8,128)(2,1)S(1)} %collective-permute-done.9.refs_0_), channel_id=1, source_target_pairs={{0,1},{1,0},{2,3},{3,2},{4,5},{5,4},{6,7},{7,6},{8,9},{9,8},{10,11... | collective-permute-start | bytes 786440 | tf_op jit(solution)/shard_map/ppermute | solution.py:40
  91.2 1.6 %copy-start.1 = (bf16[256,4096]{1,0:T(8,128)(2,1)S(1)}, bf16[256,4096]{1,0:T(8,128)(2,1)}, u32[]{:S(2)}) copy-start(bf16[256,4096]{1,0:T(8,128)(2,1)} %refs_1_.5) | copy-start | bytes 6291460
  93.4 3.0 %collective-permute-start.16 = (bf16[8,128,128]{2,1,0:T(8,128)(2,1)S(1)}, bf16[8,128,128]{2,1,0:T(8,128)(2,1)S(1)}, u32[]{:S(2)}, u32[]{:S(2)}) collective-permute-start(bf16[8,128,128]{2,1,0:T(8,128)(2,1)S(1)} %get-tuple-element.72), channel_id=1, source_target_pairs={{0,1},{1,0},{2,3},{3,2},{4,5},{5,4},{6,7},{7,6},{8,9},{9,8},{10,11... | collective-permute-start | bytes 786440 | tf_op jit(solution)/shard_map/ppermute | solution.py:40
  94.1 4.4 %collective-permute-start.20 = (bf16[8,128,128]{2,1,0:T(8,128)(2,1)S(1)}, bf16[8,128,128]{2,1,0:T(8,128)(2,1)S(1)}, u32[]{:S(2)}, u32[]{:S(2)}) collective-permute-start(bf16[8,128,128]{2,1,0:T(8,128)(2,1)S(1)} %get-tuple-element.76), channel_id=1, source_target_pairs={{0,1},{1,0},{2,3},{3,2},{4,5},{5,4},{6,7},{7,6},{8,9},{9,8},{10,11... | collective-permute-start | bytes 786440 | tf_op jit(solution)/shard_map/ppermute | solution.py:40
  95.2 4.4 %collective-permute-start.18 = (bf16[8,128,128]{2,1,0:T(8,128)(2,1)S(1)}, bf16[8,128,128]{2,1,0:T(8,128)(2,1)S(1)}, u32[]{:S(2)}, u32[]{:S(2)}) collective-permute-start(bf16[8,128,128]{2,1,0:T(8,128)(2,1)S(1)} %get-tuple-element.74), channel_id=1, source_target_pairs={{0,1},{1,0},{2,3},{3,2},{4,5},{5,4},{6,7},{7,6},{8,9},{9,8},{10,11... | collective-permute-start | bytes 786440 | tf_op jit(solution)/shard_map/ppermute | solution.py:40
  95.9 6.5 %collective-permute-start.15 = (bf16[8,128,128]{2,1,0:T(8,128)(2,1)S(1)}, bf16[8,128,128]{2,1,0:T(8,128)(2,1)S(1)}, u32[]{:S(2)}, u32[]{:S(2)}) collective-permute-start(bf16[8,128,128]{2,1,0:T(8,128)(2,1)S(1)} %get-tuple-element.70), channel_id=1, source_target_pairs={{0,1},{1,0},{2,3},{3,2},{4,5},{5,4},{6,7},{7,6},{8,9},{9,8},{10,11... | collective-permute-start | bytes 786440 | tf_op jit(solution)/shard_map/ppermute | solution.py:40
  96.5 7.4 %collective-permute-start.17 = (bf16[8,128,128]{2,1,0:T(8,128)(2,1)S(1)}, bf16[8,128,128]{2,1,0:T(8,128)(2,1)S(1)}, u32[]{:S(2)}, u32[]{:S(2)}) collective-permute-start(bf16[8,128,128]{2,1,0:T(8,128)(2,1)S(1)} %add_convert_fusion.3), channel_id=1, source_target_pairs={{0,10},{1,63},{2,8},{3,61},{4,14},{5,59},{6,12},{7,57},{8,2},{9,23... | collective-permute-start | bytes 786440 | tf_op jit(solution)/shard_map/ppermute | solution.py:81
  98.6 8.0 %collective-permute-start.21 = (bf16[8,128,128]{2,1,0:T(8,128)(2,1)S(1)}, bf16[8,128,128]{2,1,0:T(8,128)(2,1)S(1)}, u32[]{:S(2)}, u32[]{:S(2)}) collective-permute-start(bf16[8,128,128]{2,1,0:T(8,128)(2,1)S(1)} %add_convert_fusion.1), channel_id=1, source_target_pairs={{0,8},{1,57},{2,10},{3,59},{4,12},{5,61},{6,14},{7,63},{8,0},{9,17... | collective-permute-start | bytes 786440 | tf_op jit(solution)/shard_map/ppermute | solution.py:81
  99.7 6.9 %collective-permute-start.19 = (bf16[8,128,128]{2,1,0:T(8,128)(2,1)S(1)}, bf16[8,128,128]{2,1,0:T(8,128)(2,1)S(1)}, u32[]{:S(2)}, u32[]{:S(2)}) collective-permute-start(bf16[8,128,128]{2,1,0:T(8,128)(2,1)S(1)} %add_convert_fusion.2), channel_id=1, source_target_pairs={{0,2},{1,7},{2,0},{3,5},{4,6},{5,3},{6,4},{7,1},{8,10},{9,15},{10,... | collective-permute-start | bytes 786440 | tf_op jit(solution)/shard_map/ppermute | solution.py:81
